TPU v7x, 128 devices: a whole 4x4x4 slice. The times are simulated.
128 devices in a mesh: sp: 16 (over z, y), tp: 8 (over x, core).
Axes of the slice: x: 4, y: 4, z: 4, core: 2. Of those that a mesh axis runs over, the one named last changes fastest.
Arguments:
- tokens: bfloat16 [16384, 2048], P('sp', 'tp'), may hold values from -16 to 16
- mix_gain: float32 [2048], replicated, may hold values from 0.1 to 1.9
- query_weight: bfloat16 [2048, 1024], P(None, 'tp'), may hold values from -0.125 to 0.125
- key_weight: bfloat16 [2048, 1024], P(None, 'tp'), may hold values from -0.125 to 0.125
- value_weight: bfloat16 [2048, 1024], P(None, 'tp'), may hold values from -0.125 to 0.125
- outer_gate_weight: bfloat16 [2048, 1024], P(None, 'tp'), may hold values from -0.125 to 0.125
- inner_gate_weight: bfloat16 [2048, 1024], P(None, 'tp'), may hold values from -0.125 to 0.125
- conv_input_weight: bfloat16 [2048, 1024], P(None, 'tp'), may hold values from -0.125 to 0.125
- query_gain: float32 [64], replicated, may hold values from 0.6 to 10
- key_gain: float32 [64], replicated, may hold values from 0.6 to 10
- gate_totals: float32 [16384, 16], P('sp', 'tp'), may hold values from -4096 to 0, as said below
- conv_taps: float32 [3, 1024], P(None, 'tp'), may hold values from -3 to 3
- attn_out_gain: float32 [1024], P('tp'), may hold values from 0.1 to 1.9
- conv_out_gain: float32 [1024], P('tp'), may hold values from 0.1 to 1.9
- attn_out_weight: bfloat16 [1024, 2048], P('tp'), may hold values from -0.125 to 0.125
- conv_out_weight: bfloat16 [1024, 2048], P('tp'), may hold values from -0.125 to 0.125
Outputs:
- mixed: bfloat16 [16384, 2048], P(('sp', 'tp'))
Inputs may be any that keep to these rules, and one draw needn't show every extreme that they name: `gate_totals`: in every head the values never rise from one position to the next.
All inputs are finite; a program needn't handle non-finite values.
Results may differ from a plain program's by a relative error of at most 0.015.
The roundings to bfloat16 on the way count: a program that leaves them out, or rounds other values in their place, can miss the bound.
Values may be sent and summed in bfloat16 or wider, within the bound.
A program may use at most 64 MiB of HBM per device.

v0:
```python
import jax
import jax.numpy as jnp
from jax import lax
from jax.sharding import PartitionSpec as P

NORM_EPSILON = 1e-06


def sent_together(arrays, axis, dim, along):
    ends, at = ([], 0)
    for a in arrays[:-1]:
        at += a.shape[along]
        ends.append(at)
    both = jnp.concatenate(arrays, axis=along)
    return tuple(jnp.split(lax.all_gather(both, axis, axis=dim, tiled=True), ends, axis=along))


def shifted(shard, axis, by):
    devices = lax.axis_size(axis)
    pairs = [(i, i + by) for i in range(devices) if 0 <= i + by < devices]
    return lax.ppermute(shard, axis, pairs)


def head_norm(values, head_dim, gain):
    row_count = values.shape[0]
    grouped = values.reshape(row_count, -1, head_dim)
    normed = grouped * lax.rsqrt(jnp.mean(grouped * grouped, axis=2, keepdims=True) + NORM_EPSILON)
    return (normed * gain.reshape(-1, head_dim)).reshape(row_count, -1)


def per_device(
    tokens,
    mix_gain,
    query_weight,
    key_weight,
    value_weight,
    outer_gate_weight,
    inner_gate_weight,
    conv_input_weight,
    query_gain,
    key_gain,
    gate_totals,
    conv_taps,
    attn_out_gain,
    conv_out_gain,
    attn_out_weight,
    conv_out_weight,
):
    row_count = tokens.shape[0]
    head_dim = query_gain.shape[0]
    attn_width = query_weight.shape[1]
    conv_width = outer_gate_weight.shape[1]
    head_count = attn_width // head_dim
    stacked = jnp.concatenate(
        [
            query_weight,
            key_weight,
            value_weight,
            outer_gate_weight,
            inner_gate_weight,
            conv_input_weight,
        ],
        axis=1,
    )
    widened = tokens.astype(jnp.float32)
    squares = lax.psum(jnp.sum(widened * widened, axis=1), "tp")
    scaled = (
        lax.all_gather(tokens, "tp", axis=1, tiled=True).astype(jnp.float32) * mix_gain
    ).astype(jnp.bfloat16)
    product = jnp.dot(scaled, stacked, preferred_element_type=jnp.float32)
    row_scale = lax.rsqrt(squares / mix_gain.shape[0] + NORM_EPSILON)[:, None]
    projected = product * row_scale
    queries = head_norm(projected[:, 0:attn_width], head_dim, query_gain).astype(jnp.bfloat16)
    key_rows = head_norm(projected[:, attn_width : 2 * attn_width], head_dim, key_gain).astype(
        jnp.bfloat16
    )
    value_rows = projected[:, 2 * attn_width : 3 * attn_width].astype(jnp.bfloat16)
    conv_base = 3 * attn_width
    proj_outer = projected[:, conv_base : conv_base + conv_width]
    proj_inner = projected[:, conv_base + conv_width : conv_base + 2 * conv_width]
    proj_input = projected[:, conv_base + 2 * conv_width : conv_base + 3 * conv_width]
    all_gates = lax.all_gather(gate_totals, "sp", axis=0, tiled=True)
    query_start = lax.axis_index("sp") * row_count
    sp_count = lax.axis_size("sp")
    sequence_length = sp_count * row_count
    key_positions = jnp.arange(row_count, dtype=jnp.int32)
    score_scale = head_dim ** (-0.5)
    groups = [(queries, gate_totals, query_start + key_positions)]
    groups = [
        (
            group_rows.reshape(group_rows.shape[0], head_count, head_dim),
            group_gates.T,
            group_positions,
        )
        for group_rows, group_gates, group_positions in groups
    ]

    def fold_block(carried, block_keys, block_values, key_start):
        keys_heads = block_keys.reshape(row_count, head_count, head_dim)
        values_heads = block_values.reshape(row_count, head_count, head_dim)
        results = []
        for group, current_state in zip(groups, carried):
            group_queries, group_gates, group_positions = group

            def compute(
                current,
                group_queries=group_queries,
                group_gates=group_gates,
                group_positions=group_positions,
            ):
                running_max, accum = current
                scores = (
                    jnp.einsum(
                        "qhd,khd->hqk",
                        group_queries,
                        keys_heads,
                        preferred_element_type=jnp.float32,
                    )
                    * score_scale
                )
                block_gates = lax.dynamic_slice_in_dim(all_gates, key_start, row_count, 0).T
                scores = scores + group_gates[:, :, None] - block_gates[:, None, :]
                allowed = (key_start + key_positions)[None, :] <= group_positions[:, None]
                new_max = jnp.maximum(
                    running_max, jnp.max(jnp.where(allowed[None], scores, -jnp.inf), axis=2)
                )
                weights = jnp.where(
                    allowed[None], jnp.exp(scores - new_max[:, :, None]), 0.0
                ).astype(jnp.bfloat16)
                factor = jnp.exp(running_max - new_max)
                added = jnp.einsum(
                    "hqk,khd->qhd", weights, values_heads, preferred_element_type=jnp.float32
                )
                return (new_max, accum * factor.T[:, :, None] + added)

            live = (key_start >= 0) & (key_start <= group_positions[-1])
            results.append(lax.cond(live, compute, lambda current: current, current_state))
        return tuple(results)

    initial = tuple(
        (
            (
                jnp.full((head_count, group[0].shape[0]), -1e30, jnp.float32),
                jnp.zeros((group[0].shape[0], head_count, head_dim), jnp.float32),
            )
            for group in groups
        )
    )
    start_at = jnp.int32(0)
    piece_keys, piece_values = sent_together((key_rows, value_rows), "sp", 0, 1)

    def fold_one(block_number, current):
        offset = block_number * row_count
        block_keys = lax.dynamic_slice_in_dim(piece_keys, offset, row_count, 0)
        block_values = lax.dynamic_slice_in_dim(piece_values, offset, row_count, 0)
        key_start = jnp.mod(start_at + offset, sequence_length)
        return fold_block(current, block_keys, block_values, key_start)

    folded = lax.fori_loop(0, piece_keys.shape[0] // row_count, fold_one, initial)
    normed_groups = [
        head_norm(state[1].reshape(state[1].shape[0], attn_width), head_dim, attn_out_gain).astype(
            jnp.bfloat16
        )
        for state in folded
    ]
    attn_mixed = normed_groups[0]
    tap_count = conv_taps.shape[0]
    gated = (proj_inner * proj_input).astype(jnp.bfloat16)
    prior_rows = shifted(gated[row_count - tap_count + 1 :], "sp", 1)
    padded = jnp.concatenate([prior_rows, gated], axis=0).astype(jnp.float32)
    convolved = conv_taps[0] * padded[0:row_count]
    for tap_index in range(1, tap_count):
        convolved = convolved + conv_taps[tap_index] * padded[tap_index : tap_index + row_count]
    conv_mixed = head_norm(proj_outer * convolved, head_dim, conv_out_gain).astype(jnp.bfloat16)
    joined = jnp.concatenate([attn_mixed, conv_mixed], axis=1)
    out_weight = jnp.concatenate([attn_out_weight, conv_out_weight], axis=0)
    return lax.psum_scatter(
        jnp.dot(joined, out_weight, preferred_element_type=jnp.float32).astype(jnp.bfloat16),
        "tp",
        scatter_dimension=0,
        tiled=True,
    )


def solution(mesh):
    placed = (
        P("sp", "tp"),
        P(),
        P(None, "tp"),
        P(None, "tp"),
        P(None, "tp"),
        P(None, "tp"),
        P(None, "tp"),
        P(None, "tp"),
        P(),
        P(),
        P("sp", "tp"),
        P(None, "tp"),
        P("tp"),
        P("tp"),
        P("tp", None),
        P("tp", None),
    )
    return jax.shard_map(
        per_device, mesh=mesh, in_specs=placed, out_specs=P(("sp", "tp"), None), check_vma=False
    )
```

profile of v0, /device:TPU:1, one launch (start us, length us, event | category | flops | bytes accessed | tf_op | source)
XLA Modules:
  0.0 313.3 jit_solution(12489818609065645477)
XLA Ops:
  6.5 0.0 all-gather.3.cloned.1.call-start
  6.6 0.7 all-gather.3.cloned.1.call-update
  7.3 0.0 all-gather.5.cloned.1.call-start
  7.3 0.7 mul.213
  8.0 0.1 mul.214
  8.1 0.7 mul.204
  8.7 0.6 mul.205
  9.3 1.3 multiply_reduce_fusion
  10.6 13.2 %psum.7 = f32[1024]{0:T(1024)S(1)} all-reduce(f32[1024]{0:T(1024)S(1)} %multiply_reduce_fusion), channel_id=1, replica_groups=mesh['sp'=16,'tp'=8] {'tp'}, use_global_device_ids=true, to_apply=%region_1.0 | all-reduce | flops 1024 | bytes 8192 | tf_op jit(solution)/shard_map/psum | solution.py:66
  23.8 2.0 constant_dynamic-update-slice_fusion.5
  25.7 1.9 constant_dynamic-update-slice_fusion.4
  27.7 1.9 constant_dynamic-update-slice_fusion.3
  29.6 0.9 constant_dynamic-update-slice_fusion.2
  30.5 0.9 constant_dynamic-update-slice_fusion.1
  31.4 0.9 constant_dynamic-update-slice_fusion
  32.2 16.0 %all-gather.3.cloned.1.call-done = bf16[1024,2048]{1,0:T(8,128)(2,1)} async-done(((bf16[1024,256]{1,0:T(8,128)(2,1)}), bf16[1024,2048]{1,0:T(8,128)(2,1)}) %all-gather.3.cloned.1.call-update) | async-done | bytes 4194320 | tf_op jit(solution)/shard_map/all_gather | solution.py:68
  48.3 6.2 %fusion.19 = f32[1024,768]{0,1:T(8,128)S(1)} fusion(bf16[2048,768]{1,0:T(8,128)(2,1)} %constant_dynamic-update-slice_fusion, bf16[1024,2048]{1,0:T(8,128)(2,1)} %all-gather.3.cloned.1.call-done, f32[2048]{0:T(1024)S(1)} %copy-done.10, f32[1024]{0:T(1024)S(1)} %add_rsqrt_fusion.4), kind=kOutput, calls=%fused_computation.24 | convolution fusion | flops 3228303360 | bytes 10498048 | tf_op jit(solution)/shard_map/dot_general | solution.py:70
  54.5 0.0 copy-start.7
  54.5 0.0 copy-start.6
  54.5 0.1 bitcast_reduce_fusion.1
  54.7 0.9 fusion.33
  55.6 0.8 pad_maximum_fusion
  56.4 0.0 all-gather.5.cloned.1.call-update
  56.4 0.0 reduce-scatter.2.cloned.1.call-start
  56.5 0.5 slice_bitcast_fusion.2
  57.1 0.7 slice.70
  57.8 3.7 %collective-permute-start = (bf16[2,128]{0,1:T(8,128)(2,1)}, bf16[2,128]{0,1:T(8,128)(2,1)}, u32[]{:S(2)}, u32[]{:S(2)}) collective-permute-start(bf16[2,128]{0,1:T(8,128)(2,1)} %slice.70), channel_id=1, source_target_pairs={{0,8},{8,16},{16,24},{24,32},{32,40},{40,48},{48,56},{56,64},{64,7... | collective-permute-start | bytes 1544 | tf_op jit(solution)/shard_map/ppermute | solution.py:21
  61.4 19.5 %all_gather.11 = f32[16384,2]{0,1:T(2,128)S(1)} all-gather(f32[1024,2]{0,1:T(2,128)S(1)} %copy-done.6), channel_id=1, replica_groups=mesh['sp'=16,'tp'=8] {'sp'}, dimensions={0}, use_global_device_ids=true | all-gather | bytes 139264 | tf_op jit(solution)/shard_map/all_gather | solution.py:82
  80.9 1.3 mul.220
  82.3 0.9 maximum_convert_fusion
  83.2 1.1 bitcast_reduce_fusion
  84.3 0.8 fusion.31
  85.0 43.0 %all-gather.5.cloned.1.call-done = bf16[16384,256]{0,1:T(8,128)(2,1)} async-done(((bf16[1024,256]{0,1:T(8,128)(2,1)}), bf16[16384,256]{0,1:T(8,128)(2,1)}) %all-gather.5.cloned.1.call-update) | async-done | bytes 8388624 | tf_op jit(solution)/shard_map/all_gather | solution.py:15
  128.0 5.8 %fusion.38 = (bf16[16384,128]{0,1:T(8,128)(2,1)}, bf16[16384,128]{0,1:T(8,128)(2,1)}) fusion(bf16[16384,256]{0,1:T(8,128)(2,1)} %all-gather.5.cloned.1.call-done), kind=kLoop, calls=%fused_computation.75 | loop fusion | bytes 16777216 | tf_op jit(solution)/shard_map/split | solution.py:15
  133.9 0.0 copy-start.3
  133.9 0.0 copy-start.4
  133.9 28.3 %while.18 = (s32[]{:T(128)}, f32[2,1024]{1,0:T(2,128)S(1)}, f32[1024,2,64]{0,2,1:T(8,128)S(1)}, s32[1024]{0:T(1024)S(1)}, bf16[16384,128]{0,1:T(8,128)(2,1)}, /*...) while((s32[]{:T(128)}, f32[2,1024]{1,0:T(2,128)S(1)}, ...), condition=%wide.region_8.9_spmd.clone, body=%wide.region_4.8_spmd.clone.sunk | while | flops 561253376 | bytes 22934008 | solution.py:159
  133.9 0.6 slice.110
  135.2 7.2 %conditional.3 = ((f32[2,1024]{1,0:T(2,128)S(1)}, f32[1024,2,64]{0,2,1:T(8,128)S(1)})) conditional(s32[]{:T(128)} %convert_element_type.84, (f32[2,1024]{1,0:T(2,128)S(1)}, f32[1024,2,64]{0,2,1:T(8,128)S(1)}) %tuple.67, (s32[]{:T(128)}, s32[1024]{0:T(1024)S(1)}, s32[1024]{0:T(1024)S(1)}, s32[]{:T(128)}, bf16[16384,128]{0,1:T(8,128)(2,1)}, ...), branch_computations={%region_5.5_spmd, %region_6.7_spmd} | conditional | flops 561253376 | bytes 22929512 | solution.py:137
  135.2 0.1 dynamic-slice_bitcast_fusion
  135.3 0.7 broadcast_compare_fusion
  136.0 1.1 constant_dynamic-slice_fusion
  137.0 2.4 fusion.2
  139.5 2.9 fusion.12
  142.4 0.6 slice.110
  143.7 0.6 slice.110
  145.0 0.6 slice.110
  146.4 0.6 slice.110
  147.7 0.6 slice.110
  149.0 0.6 slice.110
  150.3 0.6 slice.110
  151.6 0.6 slice.110
  153.0 0.6 slice.110
  154.3 0.6 slice.110
  155.6 0.6 slice.110
  156.9 0.6 slice.110
  158.3 0.6 slice.110
  159.6 0.6 slice.110
  160.9 0.6 slice.110
  162.2 0.1 multiply_reduce_fusion.1
  162.3 0.1 multiply_convert_fusion.4
  162.4 3.2 %convolution_convert_fusion = bf16[1024,2048]{1,0:T(8,128)(2,1)} fusion(bf16[128,2048]{1,0:T(8,128)(2,1)S(1)} %copy-done.3, bf16[128,2048]{1,0:T(8,128)(2,1)S(1)} %copy-done.4, bf16[1024,128]{0,1:T(8,128)(2,1)S(1)} %fusion.31, bf16[1024,128]{0,1:T(8,128)(2,1)S(1)} %bitcast.68), kind=kOutput, calls=%fused_computation.23 | convolution fusion | flops 1078984704 | bytes 5767168 | tf_op jit(solution)/shard_map/dot_general | solution.py:178
  165.7 0.0 reduce-scatter.2.cloned.1.call-update
  165.7 141.1 %reduce-scatter.2.cloned.1.call-done = bf16[128,2048]{1,0:T(8,128)(2,1)} async-done(((bf16[1024,2048]{1,0:T(8,128)(2,1)}), bf16[128,2048]{1,0:T(8,128)(2,1)}) %reduce-scatter.2.cloned.1.call-update) | async-done | bytes 524304 | tf_op jit(solution)/shard_map/reduce_scatter | solution.py:177
  (60 shorter events, 0.5 us)
Async XLA Ops:
  6.5 23.1 %copy-start = (bf16[2048,128]{1,0:T(8,128)(2,1)S(1)}, bf16[2048,128]{1,0:T(8,128)(2,1)}, u32[]{:S(2)}) copy-start(bf16[2048,128]{1,0:T(8,128)(2,1)} %param.25) | copy-start | bytes 1572868
  6.5 24.0 %copy-start.1 = (bf16[2048,128]{1,0:T(8,128)(2,1)S(1)}, bf16[2048,128]{1,0:T(8,128)(2,1)}, u32[]{:S(2)}) copy-start(bf16[2048,128]{1,0:T(8,128)(2,1)} %param.26) | copy-start | bytes 1572868
  6.5 24.8 %copy-start.2 = (bf16[2048,128]{1,0:T(8,128)(2,1)S(1)}, bf16[2048,128]{1,0:T(8,128)(2,1)}, u32[]{:S(2)}) copy-start(bf16[2048,128]{1,0:T(8,128)(2,1)} %param.27) | copy-start | bytes 1572868
  6.5 41.7 %copy-start.10 = (f32[2048]{0:T(1024)S(1)}, f32[2048]{0:T(1024)}, u32[]{:S(2)}) copy-start(f32[2048]{0:T(1024)} %param.21) | copy-start | bytes 24580
  6.5 41.7 %all-gather.3.cloned.1.call-start = ((), (), s32[]{:S(2)}) async-start(), calls=%async_computation.1 | async-start | bytes 4718592 | tf_op jit(solution)/shard_map/all_gather | solution.py:68
  7.3 120.7 %all-gather.5.cloned.1.call-start = ((), (), s32[]{:S(2)}) async-start(), calls=%async_computation.2 | async-start | bytes 8912896 | tf_op jit(solution)/shard_map/all_gather | solution.py:15
  32.2 22.5 %copy-start.9 = (f32[128]{0:T(128)S(1)}, f32[128]{0:T(128)}, u32[]{:S(2)}) copy-start(f32[128]{0:T(128)} %mul.205) | copy-start | bytes 1540
  54.5 2.0 copy-start.7
  54.5 6.9 %copy-start.6 = (f32[1024,2]{0,1:T(2,128)S(1)}, f32[1024,2]{0,1:T(2,128)}, u32[]{:S(2)}) copy-start(f32[1024,2]{0,1:T(2,128)} %param.30) | copy-start | bytes 24580
  56.4 250.4 %reduce-scatter.2.cloned.1.call-start = ((), (), s32[]{:S(2)}) async-start(), calls=%async_computation.3 | async-start | bytes 4718592 | tf_op jit(solution)/shard_map/reduce_scatter | solution.py:177
  57.8 24.5 %collective-permute-start = (bf16[2,128]{0,1:T(8,128)(2,1)}, bf16[2,128]{0,1:T(8,128)(2,1)}, u32[]{:S(2)}, u32[]{:S(2)}) collective-permute-start(bf16[2,128]{0,1:T(8,128)(2,1)} %slice.70), channel_id=1, source_target_pairs={{0,8},{8,16},{16,24},{24,32},{32,40},{40,48},{48,56},{56,64},{64,7... | collective-permute-start | bytes 1544 | tf_op jit(solution)/shard_map/ppermute | solution.py:21
  85.0 48.8 %copy-start.5 = (bf16[1024,128]{0,1:T(8,128)(2,1)S(1)}, bf16[1024,128]{0,1:T(8,128)(2,1)}, u32[]{:S(2)}) copy-start(bf16[1024,128]{0,1:T(8,128)(2,1)} %get-tuple-element.412) | copy-start | bytes 786436
  133.9 28.4 %copy-start.8 = (f32[2,64]{1,0:T(2,128)S(1)}, f32[2,64]{1,0:T(2,128)}, u32[]{:S(2)}) copy-start(f32[2,64]{1,0:T(2,128)} %mul.220) | copy-start | bytes 1540
  133.9 28.5 %copy-start.3 = (bf16[128,2048]{1,0:T(8,128)(2,1)S(1)}, bf16[128,2048]{1,0:T(8,128)(2,1)}, u32[]{:S(2)}) copy-start(bf16[128,2048]{1,0:T(8,128)(2,1)} %param.35) | copy-start | bytes 1572868
  133.9 28.5 %copy-start.4 = (bf16[128,2048]{1,0:T(8,128)(2,1)S(1)}, bf16[128,2048]{1,0:T(8,128)(2,1)}, u32[]{:S(2)}) copy-start(bf16[128,2048]{1,0:T(8,128)(2,1)} %param.34) | copy-start | bytes 1572868
Sparse Core Ops, SparseCore 0:
  9.0 39.2 all-gather.2
  56.6 71.3 all-gather.4
  165.8 140.9 reduce-scatter.1
where the time goes:
time: 316 us; the launch traced here: 313 us
  waiting for transfers between devices  201 us (64%)
  blocking collectives  32.7 us (10%)
  local copies, waits for them, and re-layouts  29.8 us (9%)
  matrix products  14.7 us (5%)
  between operations  13.3 us (4%)
  loops' own time  11.5 us (4%)
  other arithmetic  6.66 us (2%)
  starting transfers between devices  3.81 us (1%)
    reduce_scatter x1, waiting for transfers between devices, per_device(): lax.psum_scatter(jnp.dot(joined, out_weight, preferred_element_type=jnp.f...  141 us
    all_gather x1, waiting for transfers between devices, sent_together(): lax.all_gather(both, axis, axis=dim, tiled=True)  43 us
    all_gather x1, blocking collectives, per_device(): all_gates = lax.all_gather(gate_totals, 'sp', axis=0, tiled=True)  19.5 us
    all_gather x1, waiting for transfers between devices, per_device(): lax.all_gather(tokens, 'tp', axis=1, tiled=True).astype(jnp.float32)  16 us
    psum x1, blocking collectives, per_device(): squares = lax.psum(jnp.sum(widened * widened, axis=1), 'tp')  13.2 us
    another operation x1, loops' own time, per_device(): lax.fori_loop(0, piece_keys.shape[0] // row_count, fold_one, initial)  11.2 us
    slice x16, local copies, waits for them, and re-layouts, fold_block(): live = (key_start >= 0) & (key_start <= group_positions[-1])  9.66 us
    unnamed x27, local copies, waits for them, and re-layouts  7.64 us
  transfers between devices with their start and end apart: 4, of which 3 were waited for; matrix products, arithmetic and copies ran while one was open for 5% of the time, Pallas kernels for 0%

commit v1 on v0

v1 whole, which is shorter than its diff:
```python
import functools
import math

import jax
import jax.numpy as jnp
from jax import lax
from jax.experimental import pallas as pl
from jax.experimental.pallas import tpu as pltpu
from jax.sharding import PartitionSpec as P

NORM_EPSILON = 1e-06
MESH = pl.DeviceIdType.MESH
VMEM = pltpu.VMEM
LOG2E = math.log2(math.e)
ROWS = 1024
HEAD = 64
QROWS = 80
KVROWS = 144
TILE = 512
F32 = jnp.float32
BF16 = jnp.bfloat16


def attend_kernel(
    q_ref, kv_ref, gain_ref, out_ref,
    qbuf, kvbuf, gbuf, kaug, s_ref, m_ref, acc_ref, stage,
    zsend, ysend, dsend, osend, qrecv, kvrecv, grecv, orecv,
):
    sp = lax.axis_index("sp")
    tp = lax.axis_index("tp")
    z, y = sp // 4, sp % 4
    c = tp % 2
    chip = tp - c
    zc = jnp.where((z == 1) | (z == 2), 1, 0)
    set_a = c
    set_b = 3 - c

    def dev(zz, yy, cc):
        return {"sp": zz * 4 + yy, "tp": chip + cc}

    barrier = pltpu.get_barrier_semaphore()
    for step in range(1, 8):
        other = (z * 2 + c + step) % 8
        pl.semaphore_signal(
            barrier, inc=1, device_id=dev(other // 2, y, other % 2), device_id_type=MESH
        )
    for step in (1, 3):
        pl.semaphore_signal(
            barrier, inc=1, device_id=dev(z, (y + step) % 4, c), device_id_type=MESH
        )
    pl.semaphore_wait(barrier, 9)

    qslot = z // 2
    for i in range(2):
        zt = 2 * c + i
        own = (zt == z) & (zc == c)
        pieces = (
            (kv_ref.at[i], kvbuf.at[sp], kvrecv.at[sp]),
            (q_ref.at[i], qbuf.at[qslot, pl.ds(0, QROWS)], qrecv.at[qslot]),
            (gain_ref.at[i], gbuf.at[qslot], grecv.at[qslot]),
        )

        @pl.when(own)
        def _():
            for src, dst, recv in pieces:
                pltpu.make_async_copy(src, dst, recv).start()

        @pl.when(jnp.logical_not(own))
        def _():
            for n, (src, dst, recv) in enumerate(pieces):
                pltpu.make_async_remote_copy(
                    src_ref=src, dst_ref=dst, send_sem=zsend.at[i, n], recv_sem=recv,
                    device_id=dev(zt, y, zc), device_id_type=MESH,
                ).start()

    for slot in range(2):
        qbuf[slot, QROWS:, :] = jnp.zeros((128 - QROWS, ROWS), BF16)
    m_ref[...] = jnp.full_like(m_ref, -1e30)
    acc_ref[...] = jnp.zeros_like(acc_ref)

    def arrived(b):
        pltpu.make_async_copy(kvbuf.at[b], kvbuf.at[b], kvrecv.at[b]).wait()

    def along(n, b, yy):
        pltpu.make_async_remote_copy(
            src_ref=kvbuf.at[b], dst_ref=kvbuf.at[b], send_sem=ysend.at[n],
            recv_sem=kvrecv.at[b], device_id=dev(z, yy, c), device_id_type=MESH,
        ).start()

    def across(n, b):
        pltpu.make_async_remote_copy(
            src_ref=kvbuf.at[b], dst_ref=kvbuf.at[b], send_sem=dsend.at[n],
            recv_sem=kvrecv.at[b], device_id=dev(z, y, 1 - c), device_id_type=MESH,
        ).start()

    up, down, far = (y + 1) % 4, (y + 3) % 4, (y + 2) % 4

    def share(k, ys):
        across(k, set_a * 4 + ys)

        @pl.when(c == 1)
        def _():
            across(4 + k, set_b * 4 + ys)

    own_a, own_b = set_a * 4 + y, set_b * 4 + y
    arrived(own_a)
    along(0, own_a, up)
    across(0, own_a)
    arrived(own_b)
    along(1, own_b, down)
    along(2, own_b, up)
    along(3, own_a, down)

    @pl.when(c == 1)
    def _():
        across(4, own_b)

    for slot in range(2):
        pltpu.make_async_copy(
            qbuf.at[slot, pl.ds(0, QROWS)], qbuf.at[slot, pl.ds(0, QROWS)], qrecv.at[slot]
        ).wait()
        pltpu.make_async_copy(gbuf.at[slot], gbuf.at[slot], grecv.at[slot]).wait()

    def lay_keys(b, slot):
        block = jnp.concatenate(
            [kvbuf[b, HEAD:, :], jnp.zeros((128 - QROWS, ROWS), BF16)], axis=0
        )
        kaug[slot] = block.T

    def fold(qs, b, s, tile, keys):
        at = pl.ds(tile * TILE, TILE)
        old = m_ref[qs, :, at]
        new = jnp.maximum(old, jnp.max(s, axis=0, keepdims=True))
        p = jnp.exp2(s - new).astype(BF16)
        factor = jnp.exp2(old - new)
        acc_ref[qs, :, at] = acc_ref[qs, :, at] * factor + jnp.dot(
            kvbuf[b, 0:HEAD, 0:keys], p, preferred_element_type=F32
        )
        m_ref[qs, :, at] = new

    def scores(slot, qs, tile, keys=ROWS):
        return jnp.dot(
            kaug[slot, 0:keys, :], qbuf[qs, :, pl.ds(tile * TILE, TILE)],
            preferred_element_type=F32,
        )

    def masked(s, keys):
        key = lax.broadcasted_iota(jnp.int32, (TILE, TILE), 0)
        query = lax.broadcasted_iota(jnp.int32, (TILE, TILE), 1)
        last = jnp.where(key <= query, s[keys - TILE :, :], -1e30)
        if keys == TILE:
            return last
        return jnp.concatenate([s[: keys - TILE, :], last], axis=0)

    def diagonal(n, carry):
        b = jnp.where(n == 0, own_a, own_b)
        lay_keys(b, 0)
        for tile in range(2):
            keys = (tile + 1) * TILE
            fold(n, b, masked(scores(0, n, tile, keys), keys), tile, keys)
        return carry

    lax.fori_loop(0, 2, diagonal, 0)

    def group(ys, count):
        def item(n):
            qs = jnp.where(n < 3, jnp.where((c == 1) & (n == 0), 0, 1), n - 3)
            always = jnp.where(c == 0, n, n // 2)
            zs = jnp.where(n < 3, always, jnp.where(n == 3, set_a, set_b))
            return qs, zs * 4 + ys

        qs, b = item(0)
        lay_keys(b, 0)
        s_ref[0] = scores(0, qs, 0)

        def body(n, carry):
            qs, b = item(n)
            qn, bn = item(jnp.minimum(n + 1, count - 1))
            cur = n % 2
            s_ref[1] = scores(cur, qs, 1)
            fold(qs, b, s_ref[0], 0, ROWS)
            lay_keys(bn, 1 - cur)
            s_ref[0] = scores(1 - cur, qn, 0)
            fold(qs, b, s_ref[1], 1, ROWS)
            return carry

        lax.fori_loop(0, count, body, 0)

    def shared_arrived(ys):
        @pl.when(c == 0)
        def _():
            arrived(4 + ys)
            arrived(8 + ys)

        @pl.when(c == 1)
        def _():
            arrived(ys)

    shared_arrived(y)
    group(y, 3)

    arrived(set_a * 4 + down)
    along(4, set_a * 4 + down, up)
    arrived(set_b * 4 + up)
    along(5, set_b * 4 + up, down)
    arrived(set_b * 4 + down)
    share(1, down)
    arrived(set_a * 4 + up)
    share(2, up)
    shared_arrived(down)
    group(down, jnp.where(down < y, 5, 3))
    arrived(set_a * 4 + far)
    arrived(set_b * 4 + far)
    share(3, far)
    shared_arrived(up)
    group(up, jnp.where(up < y, 5, 3))
    shared_arrived(far)
    group(far, jnp.where(far < y, 5, 3))

    for slot in range(2):
        acc = acc_ref[slot]
        scale = lax.rsqrt(jnp.mean(acc * acc, axis=0, keepdims=True) + NORM_EPSILON)
        stage[slot] = (acc * scale * gbuf[slot][:, 0:1]).astype(BF16)

    half = pl.ds(pl.multiple_of((z % 2) * HEAD, HEAD), HEAD)
    for slot in range(2):
        zt = jnp.where(slot == 0, set_a, set_b)
        own = (zt == z) & (z // 2 == c)
        dst, recv = out_ref.at[half], orecv.at[z % 2]

        @pl.when(own)
        def _():
            pltpu.make_async_copy(stage.at[slot], dst, recv).start()

        @pl.when(jnp.logical_not(own))
        def _():
            pltpu.make_async_remote_copy(
                src_ref=stage.at[slot], dst_ref=dst, send_sem=osend.at[slot], recv_sem=recv,
                device_id=dev(zt, y, z // 2), device_id_type=MESH,
            ).start()

    for i in range(2):
        zt = 2 * c + i
        own = (zt == z) & (zc == c)

        @pl.when(jnp.logical_not(own))
        def _():
            for n, src in enumerate((kv_ref.at[i], q_ref.at[i], gain_ref.at[i])):
                pltpu.make_async_copy(src, src, zsend.at[i, n]).wait()

    for n in range(6):
        pltpu.make_async_copy(kvbuf.at[0], kvbuf.at[0], ysend.at[n]).wait()
    for n in range(4):
        pltpu.make_async_copy(kvbuf.at[0], kvbuf.at[0], dsend.at[n]).wait()

    @pl.when(c == 1)
    def _():
        for n in range(4, 8):
            pltpu.make_async_copy(kvbuf.at[0], kvbuf.at[0], dsend.at[n]).wait()

    for slot in range(2):
        zt = jnp.where(slot == 0, set_a, set_b)
        own = (zt == z) & (z // 2 == c)

        @pl.when(jnp.logical_not(own))
        def _():
            pltpu.make_async_copy(stage.at[slot], stage.at[slot], osend.at[slot]).wait()

        piece = out_ref.at[pl.ds(slot * HEAD, HEAD)]
        pltpu.make_async_copy(piece, piece, orecv.at[slot]).wait()


def attend(q, kv, gain):
    DMA = pltpu.SemaphoreType.DMA
    return pl.pallas_call(
        attend_kernel,
        out_shape=jax.ShapeDtypeStruct((2 * HEAD, ROWS), BF16),
        in_specs=[pl.BlockSpec(memory_space=VMEM)] * 3,
        out_specs=pl.BlockSpec(memory_space=VMEM),
        scratch_shapes=[
            VMEM((2, 128, ROWS), BF16),
            VMEM((16, KVROWS, ROWS), BF16),
            VMEM((2, HEAD, 128), F32),
            VMEM((2, ROWS, 128), BF16),
            VMEM((2, ROWS, TILE), F32),
            VMEM((2, 1, ROWS), F32),
            VMEM((2, HEAD, ROWS), F32),
            VMEM((2, HEAD, ROWS), BF16),
            DMA((2, 3)), DMA((6,)), DMA((8,)), DMA((2,)),
            DMA((2,)), DMA((16,)), DMA((2,)), DMA((2,)),
        ],
        compiler_params=pltpu.CompilerParams(
            collective_id=1, has_side_effects=True, vmem_limit_bytes=40 * 2**20
        ),
        name="attend",
    )(q, kv, gain)


def three_parts(g):
    hi = lax.reduce_precision(g, 8, 7)
    mid = lax.reduce_precision(g - hi, 8, 7)
    low = g - hi - mid
    return jnp.stack([hi, mid, low], axis=1)


def shifted(shard, axis, by):
    devices = lax.axis_size(axis)
    pairs = [(i, i + by) for i in range(devices) if 0 <= i + by < devices]
    return lax.ppermute(shard, axis, pairs)


def norm_t(values, gain):
    grouped = values.reshape(-1, HEAD, values.shape[1])
    normed = grouped * lax.rsqrt(
        jnp.mean(grouped * grouped, axis=1, keepdims=True) + NORM_EPSILON
    )
    return normed * gain.reshape(-1, HEAD, 1)


def per_device(
    tokens, mix_gain, query_weight, key_weight, value_weight, outer_gate_weight,
    inner_gate_weight, conv_input_weight, query_gain, key_gain, gate_totals, conv_taps,
    attn_out_gain, conv_out_gain, attn_out_weight, conv_out_weight,
):
    stacked = jnp.concatenate(
        [query_weight, key_weight, value_weight, outer_gate_weight, inner_gate_weight,
         conv_input_weight], axis=1,
    )
    gathered = lax.all_gather(tokens, "tp", axis=1, tiled=True).astype(F32)
    squares = jnp.sum(gathered * gathered, axis=1)
    scaled = (gathered * mix_gain).astype(BF16)
    row_scale = lax.rsqrt(squares / mix_gain.shape[0] + NORM_EPSILON)
    projected = lax.dot_general(
        stacked, scaled, (((0,), (1,)), ((), ())), preferred_element_type=F32
    ) * row_scale[None, :]
    pq, pk, pv, po, pi, px = [projected[n * 128 : (n + 1) * 128] for n in range(6)]
    factor = LOG2E * HEAD**-0.5
    queries = norm_t(pq, jnp.tile(query_gain, 2) * factor)
    keys = norm_t(pk, jnp.tile(key_gain, 2))
    parts = three_parts(gate_totals.T * LOG2E)
    ones = jnp.ones_like(parts)
    none = jnp.zeros((2, 10, ROWS), F32)
    q = jnp.concatenate([queries, ones, parts, none], axis=1).astype(BF16)
    kv = jnp.concatenate(
        [pv.reshape(2, HEAD, ROWS), keys, -parts, ones, none], axis=1
    ).astype(BF16)
    gain = jnp.broadcast_to(attn_out_gain.reshape(2, HEAD, 1), (2, HEAD, 128))
    attn_mixed = attend(q, kv, gain)

    gated = (pi * px).astype(BF16)
    prior = shifted(gated[:, ROWS - 2 :], "sp", 1)
    padded = jnp.concatenate([prior, gated], axis=1).astype(F32)
    convolved = conv_taps[0][:, None] * padded[:, 0:ROWS]
    for tap in range(1, 3):
        convolved = convolved + conv_taps[tap][:, None] * padded[:, tap : tap + ROWS]
    conv_mixed = norm_t(po * convolved, conv_out_gain).reshape(128, ROWS).astype(BF16)
    joined = jnp.concatenate([attn_mixed, conv_mixed], axis=0)
    out_weight = jnp.concatenate([attn_out_weight, conv_out_weight], axis=0)
    return lax.psum_scatter(
        lax.dot_general(
            joined, out_weight, (((0,), (0,)), ((), ())), preferred_element_type=F32
        ).astype(BF16),
        "tp", scatter_dimension=0, tiled=True,
    )


def solution(mesh):
    placed = (
        P("sp", "tp"), P(), P(None, "tp"), P(None, "tp"), P(None, "tp"), P(None, "tp"),
        P(None, "tp"), P(None, "tp"), P(), P(), P("sp", "tp"), P(None, "tp"), P("tp"),
        P("tp"), P("tp", None), P("tp", None),
    )
    return jax.shard_map(
        per_device, mesh=mesh, in_specs=placed, out_specs=P(("sp", "tp"), None), check_vma=False
    )
```

time: 316 us -> 165 us (0.52)
  waiting for transfers between devices: 201 us -> 72.5 us
  Pallas kernels: 0 us -> 49.2 us
  blocking collectives: 32.7 us -> 0 us
  local copies, waits for them, and re-layouts: 29.8 us -> 10.2 us
  loops' own time: 11.5 us -> 0 us
  matrix products: 14.7 us -> 8.6 us
    reduce_scatter x1, waiting for transfers between devices: 141 us -> 40.5 us  [per_device(): lax.psum_scatter(lax.dot_general(joined, out_weight, (((0,), (0,)), ((),...]
    pallas_call x0 -> x1, Pallas kernels: none -> 49.2 us  [attend(): pl.pallas_call(attend_kernel, out_shape=jax.ShapeDtypeStruct((2 * HEAD, R...]
    all_gather x2 -> x1, waiting for transfers between devices: 59 us -> 30.4 us  [per_device(): gathered = lax.all_gather(tokens, 'tp', axis=1, tiled=True).astype(F32)]
    all_gather x1 -> x0, blocking collectives: 19.5 us -> none  [per_device(): all_gates = lax.all_gather(gate_totals, 'sp', axis=0, tiled=True)]
    psum x1 -> x0, blocking collectives: 13.2 us -> none  [per_device(): squares = lax.psum(jnp.sum(widened * widened, axis=1), 'tp')]
    another operation x17 -> x0, loops' own time: 11.5 us -> none  [the longest x1 11.2 us: per_device(): lax.fori_loop(0, piece_keys.shape[0] // row_count, fold_one, initial)]
    slice x18 -> x2, local copies, waits for them, and re-layouts: 10.4 us -> 0.11 us  [the longest x1 0.08 us: per_device(): prior = shifted(gated[:, ROWS - 2:], 'sp', 1)]
    dot_general x4 -> x2, matrix products: 14.7 us -> 8.6 us  [the longest x1 5.37 us: per_device(): lax.dot_general(stacked, scaled, (((0,), (1,)), ((), ())), preferred_elem...]
  transfers between devices with their start and end apart: 4 -> 3, of which waited for: 3 -> 3; matrix products, arithmetic and copies ran while one was open for 5% -> 6% of each run, Pallas kernels for 0% -> 0%
where the time goes in v1:
time: 165 us; the launch traced here: 163 us
  waiting for transfers between devices  72.5 us (44%)
  Pallas kernels  49.2 us (30%)
  between operations  13.6 us (8%)
  local copies, waits for them, and re-layouts  10.2 us (6%)
  matrix products  8.6 us (5%)
  other arithmetic  5.64 us (3%)
  starting transfers between devices  3.18 us (2%)
    pallas_call x1, Pallas kernels, attend(): pl.pallas_call(attend_kernel, out_shape=jax.ShapeDtypeStruct((2 * HEAD, R...  49.2 us
    reduce_scatter x1, waiting for transfers between devices, per_device(): lax.psum_scatter(lax.dot_general(joined, out_weight, (((0,), (0,)), ((),...  40.5 us
    all_gather x1, waiting for transfers between devices, per_device(): gathered = lax.all_gather(tokens, 'tp', axis=1, tiled=True).astype(F32)  30.4 us
    unnamed x25, local copies, waits for them, and re-layouts  6.8 us
    dot_general x1, matrix products, per_device(): lax.dot_general(stacked, scaled, (((0,), (1,)), ((), ())), preferred_elem...  5.37 us
  transfers between devices with their start and end apart: 3, of which 3 were waited for; matrix products, arithmetic and copies ran while one was open for 6% of the time, Pallas kernels for 0%

profile of v1, /device:TPU:1, one launch (start us, length us, event | category | flops | bytes accessed | tf_op | source)
XLA Modules:
  0.0 162.9 jit_solution(10825744756530940492)
XLA Ops:
  6.5 0.0 copy-start.1
  6.5 0.0 copy-start.2
  6.5 0.0 copy-start.3
  6.5 0.0 copy-start.4
  6.5 0.0 all-gather.2.cloned.1.call-start
  6.6 0.7 all-gather.2.cloned.1.call-update
  7.3 0.0 reduce-scatter.2.cloned.1.call-start
  7.3 0.7 reduce-precision_bitcast_fusion.1
  8.1 0.7 broadcast_in_dim.20
  8.9 0.7 broadcast_multiply_fusion
  9.6 0.8 slice_bitcast_fusion.2
  10.4 1.9 %constant_dynamic-update-slice_fusion.5 = bf16[2048,768]{1,0:T(8,128)(2,1)} fusion(bf16[2048,128]{1,0:T(8,128)(2,1)} %param.18), kind=kLoop, calls=%fused_computation.39 | loop fusion | bytes 1048576
  12.3 1.9 %constant_dynamic-update-slice_fusion.4 = bf16[2048,768]{1,0:T(8,128)(2,1)} fusion(bf16[2048,768]{1,0:T(8,128)(2,1)} %constant_dynamic-update-slice_fusion.5, bf16[2048,128]{1,0:T(8,128)(2,1)} %param.19), kind=kLoop, calls=%fused_computation.38 | loop fusion | bytes 1048576
  14.2 0.0 copy-done.1
  14.2 0.9 constant_dynamic-update-slice_fusion.3
  15.2 0.0 copy-done.2
  15.2 0.9 constant_dynamic-update-slice_fusion.2
  16.1 0.0 copy-done.3
  16.1 0.0 copy-start.9
  16.1 0.9 constant_dynamic-update-slice_fusion.1
  16.9 0.0 copy-done.4
  16.9 0.9 constant_dynamic-update-slice_fusion
  17.8 30.4 %all-gather.2.cloned.1.call-done = bf16[1024,2048]{1,0:T(8,128)(2,1)} async-done(((bf16[1024,256]{1,0:T(8,128)(2,1)}), bf16[1024,2048]{1,0:T(8,128)(2,1)}) %all-gather.2.cloned.1.call-update) | async-done | bytes 4194320 | tf_op jit(solution)/shard_map/all_gather | solution.py:329
  48.1 0.0 copy-start
  48.1 3.2 %fusion.1 = f32[1024]{0:T(1024)S(1)} fusion(bf16[1024,2048]{1,0:T(8,128)(2,1)} %all-gather.2.cloned.1.call-done), kind=kLoop, calls=%fused_computation.3 | loop fusion | flops 6290432 | bytes 4198400 | tf_op jit(solution)/shard_map/reduce_sum | solution.py:330
  51.4 0.0 copy-done.9
  51.4 0.2 copy-done
  51.6 5.4 %fusion.5 = f32[768,1024]{1,0:T(8,128)S(1)} fusion(bf16[2048,768]{1,0:T(8,128)(2,1)} %constant_dynamic-update-slice_fusion, bf16[1024,2048]{1,0:T(8,128)(2,1)S(1)} %copy-done, f32[2048]{0:T(1024)S(1)} %copy-done.9, f32[1024]{0:T(1024)S(1)} %add_rsqrt_fusion.3), kind=kOutput, calls=%fused_computation.7 | convolution fusion | flops 3228303360 | bytes 10498048 | tf_op jit(solution)/shard_map/dot_general | solution.py:333
  57.0 0.0 copy-start.7
  57.0 0.1 multiply_reduce_fusion
  57.1 0.1 fusion.14
  57.2 0.1 slice.59
  57.3 3.1 %collective-permute-start = (bf16[128,2]{1,0:T(8,128)(2,1)S(1)}, bf16[128,2]{1,0:T(8,128)(2,1)S(1)}, u32[]{:S(2)}, u32[]{:S(2)}) collective-permute-start(bf16[128,2]{1,0:T(8,128)(2,1)S(1)} %slice.59), channel_id=1, source_target_pairs={{0,8},{8,16},{16,24},{24,32},{32,40},{40,48},{48,56},{56,64},{64,7... | collective-permute-start | bytes 1544 | tf_op jit(solution)/shard_map/ppermute | solution.py:309
  60.4 0.9 collective-permute-done
  61.4 0.1 maximum_convert_fusion
  61.5 0.0 copy-done.7
  61.5 0.0 copy-start.8
  61.5 0.0 copy-start.5
  61.6 0.0 copy-start.6
  61.6 0.6 bitcast_reduce_fusion
  62.2 0.4 concatenate.23.kv_ref
  62.6 0.3 concatenate.22.q_ref
  62.9 0.1 broadcast_in_dim.21.gain_ref
  63.0 49.2 %attend.1 = bf16[128,1024]{1,0:T(8,128)(2,1)S(1)} custom-call(bf16[2,80,1024]{2,1,0:T(8,128)(2,1)S(1)} %concatenate.22.q_ref, bf16[2,144,1024]{2,1,0:T(8,128)(2,1)S(1)} %concatenate.23.kv_ref, f32[2,64,128]{2,1,0:T(8,128)S(1)} %broadcast_in_dim.21.gain_ref), custom_call_target="tpu_custom_call" | custom-call | tf_op jit(solution)/shard_map/attend/pallas_call | solution.py:275
  112.2 0.0 copy-done.8
  112.2 0.1 fusion.19
  112.3 0.0 copy-done.5
  112.3 0.0 copy-done.6
  112.3 3.2 %convolution_convert_fusion = bf16[1024,2048]{1,0:T(8,128)(2,1)} fusion(bf16[128,2048]{1,0:T(8,128)(2,1)S(1)} %copy-done.5, bf16[128,2048]{1,0:T(8,128)(2,1)S(1)} %copy-done.6, bf16[128,1024]{1,0:T(8,128)(2,1)S(1)} %fusion.19, bf16[128,1024]{1,0:T(8,128)(2,1)S(1)} %attend.1), kind=kOutput, calls=%fused_computation.6 | convolution fusion | flops 1078984704 | bytes 5767168 | tf_op jit(solution)/shard_map/dot_general | solution.py:360
  115.6 0.0 reduce-scatter.2.cloned.1.call-update
  115.6 40.5 %reduce-scatter.2.cloned.1.call-done = bf16[128,2048]{1,0:T(8,128)(2,1)} async-done(((bf16[1024,2048]{1,0:T(8,128)(2,1)}), bf16[128,2048]{1,0:T(8,128)(2,1)}) %reduce-scatter.2.cloned.1.call-update) | async-done | bytes 524304 | tf_op jit(solution)/shard_map/reduce_scatter | solution.py:359
  (13 shorter events, 0.2 us)
Async XLA Ops:
  6.5 7.7 %copy-start.1 = (bf16[2048,128]{1,0:T(8,128)(2,1)S(1)}, bf16[2048,128]{1,0:T(8,128)(2,1)}, u32[]{:S(2)}) copy-start(bf16[2048,128]{1,0:T(8,128)(2,1)} %param.20) | copy-start | bytes 1572868
  6.5 8.6 %copy-start.2 = (bf16[2048,128]{1,0:T(8,128)(2,1)S(1)}, bf16[2048,128]{1,0:T(8,128)(2,1)}, u32[]{:S(2)}) copy-start(bf16[2048,128]{1,0:T(8,128)(2,1)} %param.21) | copy-start | bytes 1572868
  6.5 9.5 %copy-start.3 = (bf16[2048,128]{1,0:T(8,128)(2,1)S(1)}, bf16[2048,128]{1,0:T(8,128)(2,1)}, u32[]{:S(2)}) copy-start(bf16[2048,128]{1,0:T(8,128)(2,1)} %param.22) | copy-start | bytes 1572868
  6.5 10.4 %copy-start.4 = (bf16[2048,128]{1,0:T(8,128)(2,1)S(1)}, bf16[2048,128]{1,0:T(8,128)(2,1)}, u32[]{:S(2)}) copy-start(bf16[2048,128]{1,0:T(8,128)(2,1)} %param.23) | copy-start | bytes 1572868
  6.5 41.6 %all-gather.2.cloned.1.call-start = ((), (), s32[]{:S(2)}) async-start(), calls=%async_computation.1 | async-start | bytes 4718592 | tf_op jit(solution)/shard_map/all_gather | solution.py:329
  7.3 148.8 %reduce-scatter.2.cloned.1.call-start = ((), (), s32[]{:S(2)}) async-start(), calls=%async_computation.2 | async-start | bytes 4718592 | tf_op jit(solution)/shard_map/reduce_scatter | solution.py:359
  16.1 35.3 %copy-start.9 = (f32[2048]{0:T(1024)S(1)}, f32[2048]{0:T(1024)}, u32[]{:S(2)}) copy-start(f32[2048]{0:T(1024)} %param.17) | copy-start | bytes 24580
  48.1 3.4 %copy-start = (bf16[1024,2048]{1,0:T(8,128)(2,1)S(1)}, bf16[1024,2048]{1,0:T(8,128)(2,1)}, u32[]{:S(2)}) copy-start(bf16[1024,2048]{1,0:T(8,128)(2,1)} %all-gather.2.cloned.1.call-done) | copy-start | bytes 12582916
  57.0 4.6 %copy-start.7 = (f32[64]{0:T(128)S(1)}, f32[64]{0:T(128)}, u32[]{:S(2)}) copy-start(f32[64]{0:T(128)} %param.25) | copy-start | bytes 772
  57.3 4.1 %collective-permute-start = (bf16[128,2]{1,0:T(8,128)(2,1)S(1)}, bf16[128,2]{1,0:T(8,128)(2,1)S(1)}, u32[]{:S(2)}, u32[]{:S(2)}) collective-permute-start(bf16[128,2]{1,0:T(8,128)(2,1)S(1)} %slice.59), channel_id=1, source_target_pairs={{0,8},{8,16},{16,24},{24,32},{32,40},{40,48},{48,56},{56,64},{64,7... | collective-permute-start | bytes 1544 | tf_op jit(solution)/shard_map/ppermute | solution.py:309
  61.5 50.7 %copy-start.8 = (f32[128]{0:T(128)S(1)}, f32[128]{0:T(128)}, u32[]{:S(2)}) copy-start(f32[128]{0:T(128)} %param.29) | copy-start | bytes 1540
  61.5 50.8 %copy-start.5 = (bf16[128,2048]{1,0:T(8,128)(2,1)S(1)}, bf16[128,2048]{1,0:T(8,128)(2,1)}, u32[]{:S(2)}) copy-start(bf16[128,2048]{1,0:T(8,128)(2,1)} %param.31) | copy-start | bytes 1572868
  61.6 50.8 %copy-start.6 = (bf16[128,2048]{1,0:T(8,128)(2,1)S(1)}, bf16[128,2048]{1,0:T(8,128)(2,1)}, u32[]{:S(2)}) copy-start(bf16[128,2048]{1,0:T(8,128)(2,1)} %param.30) | copy-start | bytes 1572868
Sparse Core Ops, SparseCore 0:
  9.0 39.0 all-gather.1
  115.7 40.2 reduce-scatter.1

commit v2 on v1

v2 whole, which is shorter than its diff:
```python
import math

import jax
import jax.numpy as jnp
from jax import lax
from jax.experimental import pallas as pl
from jax.experimental.pallas import tpu as pltpu
from jax.sharding import PartitionSpec as P

NORM_EPSILON = 1e-06
MESH = pl.DeviceIdType.MESH
VMEM = pltpu.VMEM
LOG2E = math.log2(math.e)
WIDTH = 2048
ROWS = 1024
CHUNK = 256
FEATURES = 256
HEAD = 64
QROWS = 80
KVROWS = 144
TILE = 512
F32 = jnp.float32
BF16 = jnp.bfloat16


def column(row):
    return jnp.broadcast_to(row, (128, 128)).T


def norm_rows(values, gain):
    scale = lax.rsqrt(jnp.mean(values * values, axis=0, keepdims=True) + NORM_EPSILON)
    return values * scale * gain


def layer_kernel(
    tokens, mix, wq, wk, wv, wo, wi, wx, qgain, kgain, gates, taps, again, cgain, wa, wc,
    out_ref,
    xbuf, wtmp, wt, xs, proj, outer, gated, halo, qout, kvout, gout, cols,
    qbuf, kvbuf, gbuf, kaug, s_ref, m_ref, acc_ref, stage, cstage, wbuf, cbuf, oacc,
    lsem, xsend, xdsend, xrecv, hsem, zsend, gsend, ysend, dsend, osend, csend, wsend,
    qrecv, kvrecv, grecv, wrecv, arecv, crecv,
):
    sp = lax.axis_index("sp")
    tp = lax.axis_index("tp")
    z, y = sp // 4, sp % 4
    x, c = tp // 2, tp % 2
    zc = jnp.where((z == 1) | (z == 2), 1, 0)
    set_a = c
    set_b = 3 - c

    def dev(zz, yy, xx, cc):
        return {"sp": zz * 4 + yy, "tp": xx * 2 + cc}

    def local(src, dst, sem):
        return pltpu.make_async_copy(src, dst, sem)

    def remote(src, dst, send, recv, to):
        return pltpu.make_async_remote_copy(
            src_ref=src, dst_ref=dst, send_sem=send, recv_sem=recv, device_id=to,
            device_id_type=MESH,
        )

    def drain(ref, sem):
        pltpu.make_async_copy(ref, ref, sem).wait()

    mine = local(tokens, xbuf.at[tp], lsem.at[0])
    mine.start()
    weights = [
        local(w, wtmp.at[n], lsem.at[1 + n]) for n, w in enumerate((wq, wk, wv, wo, wi, wx))
    ]
    for w in weights:
        w.start()
    own_wa = pl.ds(pl.multiple_of(tp * 128, 128), 128)
    own_wc = pl.ds(pl.multiple_of(1024 + tp * 128, 128), 128)
    out_a = local(wa, wbuf.at[own_wa], lsem.at[7])
    out_c = local(wc, wbuf.at[own_wc], lsem.at[8])
    out_a.start()
    out_c.start()

    barrier = pltpu.get_barrier_semaphore()

    def greet(step, carry):
        other = (z * 8 + tp + step) % 32
        pl.semaphore_signal(
            barrier, inc=1, device_id={"sp": (other // 8) * 4 + y, "tp": other % 8},
            device_id_type=MESH,
        )
        return carry

    lax.fori_loop(1, 32, greet, 0)
    for step in (1, 3):
        pl.semaphore_signal(
            barrier, inc=1, device_id=dev(z, (y + step) % 4, x, c), device_id_type=MESH
        )
    for step in (1, 15):
        pl.semaphore_signal(
            barrier, inc=1, device_id={"sp": (sp + step) % 16, "tp": tp}, device_id_type=MESH
        )
    mine.wait()
    pl.semaphore_wait(barrier, 35)

    right, left, across_x = (x + 1) % 4, (x + 3) % 4, (x + 2) % 4
    sib = dev(z, y, x, 1 - c)

    def rows(t, n, half=None):
        if half is None:
            return xbuf.at[t, pl.ds(pl.multiple_of(n * CHUNK, CHUNK), CHUNK)]
        return xbuf.at[t, pl.ds(pl.multiple_of(n * CHUNK + half * 128, 128), 128)]

    def send_own(n):
        piece = rows(tp, n)
        remote(piece, piece, xsend.at[0, n], xrecv.at[tp, n], dev(z, y, right, c)).start()
        remote(piece, piece, xsend.at[1, n], xrecv.at[tp, n], dev(z, y, left, c)).start()
        remote(piece, piece, xdsend.at[0, n], xrecv.at[tp, n], sib).start()

    send_own(0)
    send_own(1)

    for n, row in enumerate((qgain, kgain)):
        both = jnp.concatenate([row[...], row[...]], axis=1)
        if n == 0:
            both = both * (LOG2E * HEAD**-0.5)
        cols[n] = column(both)
    for n in range(3):
        cols[2 + n] = column(taps[n : n + 1, :])
    cols[5] = column(cgain[...])
    out_gain = column(again[...])
    for i in range(2):
        gout[i] = out_gain[i * HEAD : (i + 1) * HEAD]
    spot = lax.broadcasted_iota(jnp.int32, (16, ROWS), 0)
    for i in range(2):
        g = gates[i : i + 1, :] * LOG2E
        hi = g.astype(BF16).astype(F32)
        mid = (g - hi).astype(BF16).astype(F32)
        low = g - hi - mid
        one = jnp.where(spot < 3, 1.0, 0.0)
        parts = jnp.where(spot == 3, hi, jnp.where(spot == 4, mid, jnp.where(spot == 5, low, one)))
        qout[i, HEAD:, :] = parts.astype(BF16)
        one = jnp.where((spot > 2) & (spot < 6), 1.0, 0.0)
        parts = jnp.where(spot == 0, -hi, jnp.where(spot == 1, -mid, jnp.where(spot == 2, -low, one)))
        kvout[i, 2 * HEAD :, :] = parts.astype(BF16)
    for n, w in enumerate(weights):
        w.wait()
        for k in range(4):
            wt[n * 128 : (n + 1) * 128, k * 512 : (k + 1) * 512] = wtmp[
                n, k * 512 : (k + 1) * 512, :
            ].T

    for slot in range(2):
        qbuf[slot, QROWS:, :] = jnp.zeros((128 - QROWS, ROWS), BF16)
    m_ref[...] = jnp.full_like(m_ref, -1e30)
    acc_ref[...] = jnp.zeros_like(acc_ref)

    @pl.when(sp == 0)
    def _():
        halo[...] = jnp.zeros_like(halo)

    qslot = z // 2

    def z_sends(n):
        at = pl.ds(pl.multiple_of(n * CHUNK, CHUNK), CHUNK)
        for i in range(2):
            zt = 2 * c + i
            own = (zt == z) & (zc == c)
            pieces = (
                (kvout.at[i, :, at], kvbuf.at[sp, :, at], kvrecv.at[sp]),
                (qout.at[i, :, at], qbuf.at[qslot, pl.ds(0, QROWS), at], qrecv.at[qslot]),
            )

            @pl.when(own)
            def _():
                for src, dst, recv in pieces:
                    local(src, dst, recv).start()

            @pl.when(jnp.logical_not(own))
            def _():
                for k, (src, dst, recv) in enumerate(pieces):
                    remote(src, dst, zsend.at[i, k, n], recv, dev(zt, y, x, zc)).start()

    for i in range(2):
        zt = 2 * c + i
        own = (zt == z) & (zc == c)

        @pl.when(own)
        def _():
            local(gout.at[i], gbuf.at[qslot], grecv.at[qslot]).start()

        @pl.when(jnp.logical_not(own))
        def _():
            remote(
                gout.at[i], gbuf.at[qslot], gsend.at[i], grecv.at[qslot], dev(zt, y, x, zc)
            ).start()

    def project(n):
        at = pl.ds(pl.multiple_of(n * CHUNK, CHUNK), CHUNK)
        squares = jnp.zeros((CHUNK, 128), F32)
        for t in range(8):
            piece = xbuf[t, at, :].astype(F32)
            squares = squares + piece[:, :128] * piece[:, :128] + piece[:, 128:] * piece[:, 128:]
            lanes = slice(t * FEATURES, (t + 1) * FEATURES)
            xs[:, lanes] = (piece * mix[:, lanes]).astype(BF16)
        total = jnp.sum(squares.T, axis=0, keepdims=True)
        row_scale = lax.rsqrt(total / WIDTH + NORM_EPSILON)
        proj[...] = lax.dot_general(
            wt[...], xs[...], (((1,), (1,)), ((), ())), preferred_element_type=F32
        ) * row_scale
        for i in range(2):
            lo = i * HEAD
            wide = [
                jnp.concatenate([cols[k, lo : lo + HEAD]] * 2, axis=1) for k in range(2)
            ]
            qout[i, 0:HEAD, at] = norm_rows(proj[lo : lo + HEAD], wide[0]).astype(BF16)
            kvout[i, HEAD : 2 * HEAD, at] = norm_rows(
                proj[128 + lo : 128 + lo + HEAD], wide[1]
            ).astype(BF16)
            kvout[i, 0:HEAD, at] = proj[256 + lo : 256 + lo + HEAD].astype(BF16)
        outer[:, at] = proj[384:512]
        gated[:, at] = (proj[512:640] * proj[640:768]).astype(BF16)

    def gather(n, carry):
        @pl.when(n < 4)
        def _():
            before, after = left * 2 + c, right * 2 + c
            drain(rows(before, n), xrecv.at[before, n])
            piece = rows(before, n, 0)
            remote(piece, piece, xsend.at[2, n], xrecv.at[before, n], dev(z, y, right, c)).start()
            piece = rows(before, n)
            remote(piece, piece, xdsend.at[1, n], xrecv.at[before, n], sib).start()
            drain(rows(after, n), xrecv.at[after, n])
            piece = rows(after, n, 1)
            remote(piece, piece, xsend.at[3, n], xrecv.at[after, n], dev(z, y, left, c)).start()
            piece = rows(after, n)
            remote(piece, piece, xdsend.at[2, n], xrecv.at[after, n], sib).start()

            @pl.when(n < 2)
            def _():
                send_own(n + 2)

        @pl.when(n > 0)
        def _():
            done = n - 1
            far = across_x * 2 + c
            drain(rows(far, done), xrecv.at[far, done])
            piece = rows(far, done)
            remote(piece, piece, xdsend.at[3, done], xrecv.at[far, done], sib).start()
            for xx in range(4):
                t = xx * 2 + 1 - c
                drain(rows(t, done), xrecv.at[t, done])
            project(done)
            z_sends(done)

        return carry

    lax.fori_loop(0, 5, gather, 0)

    @pl.when(sp < 15)
    def _():
        remote(
            gated.at[:, pl.ds(ROWS - 128, 128)], halo, hsem.at[0], hsem.at[1],
            {"sp": jnp.minimum(sp + 1, 15), "tp": tp},
        ).start()

    def w_rows(t, kind):
        return pl.ds(pl.multiple_of(kind * 1024 + t * 128, 128), 128)

    def w_send(n, t, kind, to):
        piece = wbuf.at[w_rows(t, kind)]
        remote(piece, piece, wsend.at[n], wrecv.at[kind * 8 + t], to).start()

    def w_wait(t, kind):
        drain(wbuf.at[w_rows(t, kind)], wrecv.at[kind * 8 + t])

    out_a.wait()
    out_c.wait()
    w_send(0, tp, 0, dev(z, y, right, c))
    w_send(1, tp, 1, dev(z, y, left, c))
    w_send(2, tp, 1, dev(z, y, right, c))
    w_send(3, tp, 0, dev(z, y, left, c))
    w_send(4, tp, 0, sib)
    w_send(5, tp, 1, sib)

    def mix_conv():
        prior = jnp.concatenate([halo[...], gated[...]], axis=1).astype(F32)
        conv = jnp.concatenate([cols[4]] * 8, axis=1) * prior[:, 128:]
        for tap in range(2):
            moved = pltpu.roll(prior, 2 - tap, axis=1)
            conv = conv + jnp.concatenate([cols[2 + tap]] * 8, axis=1) * moved[:, 128:]
        value = outer[...] * conv
        for i in range(2):
            part = slice(i * HEAD, (i + 1) * HEAD)
            wide = jnp.concatenate([cols[5, part]] * 8, axis=1)
            cstage[part, :] = norm_rows(value[part], wide).astype(BF16)

    @pl.when(sp > 0)
    def _():
        drain(halo, hsem.at[1])

    mix_conv()
    to_rows = pl.ds(pl.multiple_of(1024 + tp * 128, 128), 128)
    local(
        cstage.at[:, pl.ds(pl.multiple_of(tp * 128, 128), 128)], cbuf.at[to_rows], crecv.at[tp]
    ).start()
    for step in range(1, 8):
        t = (tp + step) % 8
        remote(
            cstage.at[:, pl.ds(pl.multiple_of(t * 128, 128), 128)], cbuf.at[to_rows],
            csend.at[step], crecv.at[tp], {"sp": sp, "tp": t},
        ).start()

    def arrived(b):
        pltpu.make_async_copy(kvbuf.at[b], kvbuf.at[b], kvrecv.at[b]).wait()

    def along(n, b, yy):
        pltpu.make_async_remote_copy(
            src_ref=kvbuf.at[b], dst_ref=kvbuf.at[b], send_sem=ysend.at[n],
            recv_sem=kvrecv.at[b], device_id=dev(z, yy, x, c), device_id_type=MESH,
        ).start()

    def across(n, b):
        pltpu.make_async_remote_copy(
            src_ref=kvbuf.at[b], dst_ref=kvbuf.at[b], send_sem=dsend.at[n],
            recv_sem=kvrecv.at[b], device_id=sib, device_id_type=MESH,
        ).start()

    up, down, far = (y + 1) % 4, (y + 3) % 4, (y + 2) % 4

    def share(k, ys):
        across(k, set_a * 4 + ys)

        @pl.when(c == 1)
        def _():
            across(4 + k, set_b * 4 + ys)

    own_a, own_b = set_a * 4 + y, set_b * 4 + y
    arrived(own_a)
    along(0, own_a, up)
    across(0, own_a)
    arrived(own_b)
    along(1, own_b, down)
    along(2, own_b, up)
    along(3, own_a, down)

    @pl.when(c == 1)
    def _():
        across(4, own_b)

    for slot in range(2):
        pltpu.make_async_copy(
            qbuf.at[slot, pl.ds(0, QROWS)], qbuf.at[slot, pl.ds(0, QROWS)], qrecv.at[slot]
        ).wait()
        pltpu.make_async_copy(gbuf.at[slot], gbuf.at[slot], grecv.at[slot]).wait()

    def lay_keys(b, slot):
        block = jnp.concatenate(
            [kvbuf[b, HEAD:, :], jnp.zeros((128 - QROWS, ROWS), BF16)], axis=0
        )
        kaug[slot] = block.T

    def fold(qs, b, s, tile, keys):
        at = pl.ds(tile * TILE, TILE)
        old = m_ref[qs, :, at]
        new = jnp.maximum(old, jnp.max(s, axis=0, keepdims=True))
        p = jnp.exp2(s - new).astype(BF16)
        factor = jnp.exp2(old - new)
        acc_ref[qs, :, at] = acc_ref[qs, :, at] * factor + jnp.dot(
            kvbuf[b, 0:HEAD, 0:keys], p, preferred_element_type=F32
        )
        m_ref[qs, :, at] = new

    def scores(slot, qs, tile, keys=ROWS):
        return jnp.dot(
            kaug[slot, 0:keys, :], qbuf[qs, :, pl.ds(tile * TILE, TILE)],
            preferred_element_type=F32,
        )

    def masked(s, keys):
        key = lax.broadcasted_iota(jnp.int32, (TILE, TILE), 0)
        query = lax.broadcasted_iota(jnp.int32, (TILE, TILE), 1)
        last = jnp.where(key <= query, s[keys - TILE :, :], -1e30)
        if keys == TILE:
            return last
        return jnp.concatenate([s[: keys - TILE, :], last], axis=0)

    def diagonal(n, carry):
        b = jnp.where(n == 0, own_a, own_b)
        lay_keys(b, 0)
        for tile in range(2):
            keys = (tile + 1) * TILE
            fold(n, b, masked(scores(0, n, tile, keys), keys), tile, keys)
        return carry

    lax.fori_loop(0, 2, diagonal, 0)

    def group(ys, count):
        def item(n):
            qs = jnp.where(n < 3, jnp.where((c == 1) & (n == 0), 0, 1), n - 3)
            always = jnp.where(c == 0, n, n // 2)
            zs = jnp.where(n < 3, always, jnp.where(n == 3, set_a, set_b))
            return qs, zs * 4 + ys

        qs, b = item(0)
        lay_keys(b, 0)
        s_ref[0] = scores(0, qs, 0)

        def body(n, carry):
            qs, b = item(n)
            qn, bn = item(jnp.minimum(n + 1, count - 1))
            cur = n % 2
            s_ref[1] = scores(cur, qs, 1)
            fold(qs, b, s_ref[0], 0, ROWS)
            lay_keys(bn, 1 - cur)
            s_ref[0] = scores(1 - cur, qn, 0)
            fold(qs, b, s_ref[1], 1, ROWS)
            return carry

        lax.fori_loop(0, count, body, 0)

    def shared_arrived(ys):
        @pl.when(c == 0)
        def _():
            arrived(4 + ys)
            arrived(8 + ys)

        @pl.when(c == 1)
        def _():
            arrived(ys)

    shared_arrived(y)
    group(y, 3)
    before, after, far_x = left * 2 + c, right * 2 + c, across_x * 2 + c

    arrived(set_a * 4 + down)
    along(4, set_a * 4 + down, up)
    arrived(set_b * 4 + up)
    along(5, set_b * 4 + up, down)
    arrived(set_b * 4 + down)
    share(1, down)
    arrived(set_a * 4 + up)
    share(2, up)
    shared_arrived(down)
    group(down, jnp.where(down < y, 5, 3))
    w_wait(before, 0)
    w_send(6, before, 0, dev(z, y, right, c))
    w_send(7, before, 0, sib)
    w_wait(after, 1)
    w_send(8, after, 1, dev(z, y, left, c))
    w_send(9, after, 1, sib)
    arrived(set_a * 4 + far)
    arrived(set_b * 4 + far)
    share(3, far)
    shared_arrived(up)
    group(up, jnp.where(up < y, 5, 3))
    w_wait(before, 1)
    w_send(10, before, 1, sib)
    w_wait(after, 0)
    w_send(11, after, 0, sib)
    shared_arrived(far)
    group(far, jnp.where(far < y, 5, 3))

    for slot in range(2):
        stage[slot] = norm_rows(acc_ref[slot], gbuf[slot][:, 0:1]).astype(BF16)
        head = x * 4 + z
        dst = cbuf.at[pl.ds(pl.multiple_of(head * HEAD, HEAD), HEAD)]
        zt = jnp.where(slot == 0, set_a, set_b)
        for step in range(8):
            t = (tp + step) % 8
            piece = stage.at[slot, :, pl.ds(pl.multiple_of(t * 128, 128), 128)]
            if step:
                remote(
                    piece, dst, osend.at[slot, step], arecv.at[head],
                    {"sp": zt * 4 + y, "tp": t},
                ).start()
                continue

            @pl.when(zt == z)
            def _():
                local(piece, dst, arecv.at[head]).start()

            @pl.when(zt != z)
            def _():
                remote(
                    piece, dst, osend.at[slot, step], arecv.at[head],
                    {"sp": zt * 4 + y, "tp": t},
                ).start()

    w_wait(far_x, 0)
    w_send(12, far_x, 0, sib)
    w_wait(far_x, 1)
    w_send(13, far_x, 1, sib)
    for xx in range(4):
        w_wait(xx * 2 + 1 - c, 0)
        w_wait(xx * 2 + 1 - c, 1)
    for t in range(8):
        drain(cbuf.at[pl.ds(1024 + t * 128, 128)], crecv.at[t])

    def product(lo, n):
        at = pl.ds(pl.multiple_of(n * TILE, TILE), TILE)
        return jnp.dot(
            cbuf[lo : lo + 1024, :].T, wbuf[lo : lo + 1024, at], preferred_element_type=F32
        )

    def conv_part(n, carry):
        oacc[:, pl.ds(pl.multiple_of(n * TILE, TILE), TILE)] = product(1024, n)
        return carry

    lax.fori_loop(0, WIDTH // TILE, conv_part, 0)
    for h in range(16):
        drain(cbuf.at[pl.ds(h * HEAD, HEAD)], arecv.at[h])

    def attn_part(n, carry):
        at = pl.ds(pl.multiple_of(n * TILE, TILE), TILE)
        out_ref[:, at] = (oacc[:, at] + product(0, n)).astype(BF16)
        return carry

    lax.fori_loop(0, WIDTH // TILE, attn_part, 0)

    def sent(n, carry):
        for k in range(2):
            drain(rows(tp, n), xsend.at[k, n])
            drain(rows(tp, n, 0), xsend.at[2 + k, n])
        for k in range(4):
            drain(rows(tp, n), xdsend.at[k, n])
        for i in range(2):
            zt = 2 * c + i
            own = (zt == z) & (zc == c)
            at = pl.ds(pl.multiple_of(n * CHUNK, CHUNK), CHUNK)

            @pl.when(jnp.logical_not(own))
            def _():
                drain(kvout.at[i, :, at], zsend.at[i, 0, n])
                drain(qout.at[i, :, at], zsend.at[i, 1, n])

        return carry

    lax.fori_loop(0, 4, sent, 0)
    for i in range(2):
        zt = 2 * c + i
        own = (zt == z) & (zc == c)

        @pl.when(jnp.logical_not(own))
        def _():
            drain(gout.at[i], gsend.at[i])

    @pl.when(sp < 15)
    def _():
        drain(halo, hsem.at[0])

    for n in range(6):
        drain(kvbuf.at[0], ysend.at[n])
    for n in range(4):
        drain(kvbuf.at[0], dsend.at[n])

    @pl.when(c == 1)
    def _():
        for n in range(4, 8):
            drain(kvbuf.at[0], dsend.at[n])

    for n in range(14):
        drain(wbuf.at[pl.ds(0, 128)], wsend.at[n])
    for step in range(1, 8):
        drain(cbuf.at[pl.ds(0, 128)], csend.at[step])
    for slot in range(2):
        zt = jnp.where(slot == 0, set_a, set_b)
        piece = stage.at[slot, :, pl.ds(0, 128)]
        for step in range(1, 8):
            drain(piece, osend.at[slot, step])

        @pl.when(zt != z)
        def _():
            drain(piece, osend.at[slot, 0])


def per_device(
    tokens, mix_gain, query_weight, key_weight, value_weight, outer_gate_weight,
    inner_gate_weight, conv_input_weight, query_gain, key_gain, gate_totals, conv_taps,
    attn_out_gain, conv_out_gain, attn_out_weight, conv_out_weight,
):
    DMA = pltpu.SemaphoreType.DMA
    far = pl.BlockSpec(memory_space=pl.ANY)
    near = pl.BlockSpec(memory_space=VMEM)
    return pl.pallas_call(
        layer_kernel,
        out_shape=jax.ShapeDtypeStruct((128, WIDTH), BF16),
        in_specs=[far, near] + [far] * 6 + [near] * 6 + [far] * 2,
        out_specs=near,
        scratch_shapes=[
            VMEM((8, ROWS, FEATURES), BF16),
            VMEM((6, WIDTH, 128), BF16),
            VMEM((768, WIDTH), BF16),
            VMEM((CHUNK, WIDTH), BF16),
            VMEM((768, CHUNK), F32),
            VMEM((128, ROWS), F32),
            VMEM((128, ROWS), BF16),
            VMEM((128, 128), BF16),
            VMEM((2, QROWS, ROWS), BF16),
            VMEM((2, KVROWS, ROWS), BF16),
            VMEM((2, HEAD, 128), F32),
            VMEM((6, 128, 128), F32),
            VMEM((2, 128, ROWS), BF16),
            VMEM((16, KVROWS, ROWS), BF16),
            VMEM((2, HEAD, 128), F32),
            VMEM((2, ROWS, 128), BF16),
            VMEM((2, ROWS, TILE), F32),
            VMEM((2, 1, ROWS), F32),
            VMEM((2, HEAD, ROWS), F32),
            VMEM((2, HEAD, ROWS), BF16),
            VMEM((128, ROWS), BF16),
            VMEM((WIDTH, WIDTH), BF16),
            VMEM((WIDTH, 128), BF16),
            VMEM((128, WIDTH), F32),
            DMA((9,)), DMA((4, 4)), DMA((4, 4)), DMA((8, 4)), DMA((2,)),
            DMA((2, 2, 4)), DMA((2,)), DMA((6,)), DMA((8,)), DMA((2, 8)), DMA((8,)), DMA((14,)),
            DMA((2,)), DMA((16,)), DMA((2,)), DMA((16,)), DMA((16,)), DMA((8,)),
        ],
        compiler_params=pltpu.CompilerParams(
            collective_id=1, has_side_effects=True, vmem_limit_bytes=56 * 2**20
        ),
        name="layer",
    )(
        tokens, mix_gain.reshape(1, WIDTH), query_weight, key_weight, value_weight,
        outer_gate_weight, inner_gate_weight, conv_input_weight, query_gain.reshape(1, HEAD),
        key_gain.reshape(1, HEAD), gate_totals.T, conv_taps, attn_out_gain.reshape(1, 128),
        conv_out_gain.reshape(1, 128), attn_out_weight, conv_out_weight,
    )


def solution(mesh):
    placed = (
        P("sp", "tp"), P(), P(None, "tp"), P(None, "tp"), P(None, "tp"), P(None, "tp"),
        P(None, "tp"), P(None, "tp"), P(), P(), P("sp", "tp"), P(None, "tp"), P("tp"),
        P("tp"), P("tp", None), P("tp", None),
    )
    return jax.shard_map(
        per_device, mesh=mesh, in_specs=placed, out_specs=P(("sp", "tp"), None), check_vma=False
    )
```

time: 165 us -> 81.9 us (0.50); the launches traced: 163 us -> 81.7 us
  waiting for transfers between devices: 72.5 us -> 0 us
  Pallas kernels: 49.2 us -> 79.8 us
  between operations: 13.6 us -> 0.01 us
  matrix products: 8.6 us -> 0 us
  local copies, waits for them, and re-layouts: 10.2 us -> 1.88 us
  other arithmetic: 5.64 us -> 0 us
  starting transfers between devices: 3.18 us -> 0 us
    reduce_scatter x1 -> x0, waiting for transfers between devices: 40.5 us -> none  [per_device(): lax.psum_scatter(lax.dot_general(joined, out_weight, (((0,), (0,)), ((),...]
    pallas_call x1, Pallas kernels: 49.2 us -> 79.8 us  [per_device(): pl.pallas_call(layer_kernel, out_shape=jax.ShapeDtypeStruct((128, WIDTH),...]
    all_gather x1 -> x0, waiting for transfers between devices: 30.4 us -> none  [per_device(): gathered = lax.all_gather(tokens, 'tp', axis=1, tiled=True).astype(F32)]
    dot_general x2 -> x0, matrix products: 8.6 us -> none  [the longest x1 5.37 us: per_device(): lax.dot_general(stacked, scaled, (((0,), (1,)), ((), ())), preferred_elem...]
    unnamed x25 -> x1, local copies, waits for them, and re-layouts: 6.8 us -> 1.88 us
    reduce_sum x3 -> x0, other arithmetic: 3.89 us -> none  [the longest x1 3.22 us: per_device(): squares = jnp.sum(gathered * gathered, axis=1)]
    ppermute x1 -> x0, starting transfers between devices: 3.1 us -> none  [shifted(): return lax.ppermute(shard, axis, pairs)]
  transfers between devices with their start and end apart: 3 -> 0, of which waited for: 3 -> 0; matrix products, arithmetic and copies ran while one was open for 6% -> 0% of each run, Pallas kernels for 0% -> 0%
where the time goes in v2:
time: 81.9 us; the launch traced here: 81.7 us
  Pallas kernels  79.8 us (97%)
  local copies, waits for them, and re-layouts  1.88 us (2%)
    pallas_call x1, Pallas kernels, per_device(): pl.pallas_call(layer_kernel, out_shape=jax.ShapeDtypeStruct((128, WIDTH),...  79.8 us
    unnamed x1, local copies, waits for them, and re-layouts  1.88 us

profile of v2, /device:TPU:1, one launch (start us, length us, event | category | flops | bytes accessed | tf_op | source)
XLA Modules:
  0.0 81.7 jit_solution(6662243612427497026)
XLA Ops:
  0.0 79.8 %layer.1 = bf16[128,2048]{1,0:T(8,128)(2,1)} custom-call(bf16[1024,256]{1,0:T(8,128)(2,1)} %tokens.1, f32[1,2048]{1,0:T(1,128)} %bitcast.6, bf16[2048,128]{1,0:T(8,128)(2,1)} %wq.1, bf16[2048,128]{1,0:T(8,128)(2,1)} %wk.1, bf16[2048,128]{1,0:T(8,128)(2,1)} %wv.1, bf16[2048,128]{1,0:T(8,128)(2,1)} %wo.1, bf16[2048,128]{1,0:T(8,128)(2,1)} %wi.1, ...), custom_call_target="tpu_custom_call" | custom-call | tf_op jit(solution)/shard_map/layer/pallas_call | solution.py:581
  79.9 1.9 %copy.18 = bf16[128,2048]{1,0:T(8,128)(2,1)} copy(bf16[128,2048]{1,0:T(8,128)(2,1)} %layer.1) | data formatting | bytes 1048576

commit v3 on v2

--- a/solution.py
+++ b/solution.py
@@ -35,10 +35,10 @@
 def layer_kernel(
     tokens, mix, wq, wk, wv, wo, wi, wx, qgain, kgain, gates, taps, again, cgain, wa, wc,
     out_ref,
-    xbuf, wtmp, wt, xs, proj, outer, gated, halo, qout, kvout, gout, cols,
-    qbuf, kvbuf, gbuf, kaug, s_ref, m_ref, acc_ref, stage, cstage, wbuf, cbuf, oacc,
-    lsem, xsend, xdsend, xrecv, hsem, zsend, gsend, ysend, dsend, osend, csend, wsend,
-    qrecv, kvrecv, grecv, wrecv, arecv, crecv,
+    xbuf, wtmp, wt, xs, scale_ref, proj, outer, gated, halo, qout, kvout, gout, cols,
+    qbuf, kvbuf, gbuf, kaug, s_ref, m_ref, acc_ref, stage, cstage, wbuf, cbuf, ct, oacc,
+    lsem, xsend, xdsend, xrecv, hsem, zsend, gsend, ysend, dsend, osend, csend, wsend, hsend,
+    qrecv, kvrecv, grecv, wrecv, hrecv, arecv, crecv,
 ):
     sp = lax.axis_index("sp")
     tp = lax.axis_index("tp")
@@ -163,8 +163,8 @@
             zt = 2 * c + i
             own = (zt == z) & (zc == c)
             pieces = (
-                (kvout.at[i, :, at], kvbuf.at[sp, :, at], kvrecv.at[sp]),
-                (qout.at[i, :, at], qbuf.at[qslot, pl.ds(0, QROWS), at], qrecv.at[qslot]),
+                (kvout.at[i, :, at], kvbuf.at[sp, :, at], kvrecv.at[sp, n]),
+                (qout.at[i, :, at], qbuf.at[qslot, pl.ds(0, QROWS), at], qrecv.at[qslot, n]),
             )
 
             @pl.when(own)
@@ -201,8 +201,9 @@
             xs[:, lanes] = (piece * mix[:, lanes]).astype(BF16)
         total = jnp.sum(squares.T, axis=0, keepdims=True)
         row_scale = lax.rsqrt(total / WIDTH + NORM_EPSILON)
-        proj[...] = lax.dot_general(
-            wt[...], xs[...], (((1,), (1,)), ((), ())), preferred_element_type=F32
+        scale_ref[...] = row_scale
+        proj[0:384] = lax.dot_general(
+            wt[0:384], xs[...], (((1,), (1,)), ((), ())), preferred_element_type=F32
         ) * row_scale
         for i in range(2):
             lo = i * HEAD
@@ -214,13 +215,158 @@
                 proj[128 + lo : 128 + lo + HEAD], wide[1]
             ).astype(BF16)
             kvout[i, 0:HEAD, at] = proj[256 + lo : 256 + lo + HEAD].astype(BF16)
+
+    def project_conv(n):
+        at = pl.ds(pl.multiple_of(n * CHUNK, CHUNK), CHUNK)
+        proj[384:768] = lax.dot_general(
+            wt[384:768], xs[...], (((1,), (1,)), ((), ())), preferred_element_type=F32
+        ) * scale_ref[...]
         outer[:, at] = proj[384:512]
         gated[:, at] = (proj[512:640] * proj[640:768]).astype(BF16)
 
+    def chunk(b, k):
+        return kvbuf.at[b, :, pl.ds(pl.multiple_of(k * CHUNK, CHUNK), CHUNK)]
+
+    def arrived(b, k):
+        drain(chunk(b, k), kvrecv.at[b, k])
+
+    def along(n, b, k, yy):
+        piece = chunk(b, k)
+        remote(piece, piece, ysend.at[n, k], kvrecv.at[b, k], dev(z, yy, x, c)).start()
+
+    def across(n, b, k):
+        piece = chunk(b, k)
+        remote(piece, piece, dsend.at[n, k], kvrecv.at[b, k], sib).start()
+
+    up, down, far = (y + 1) % 4, (y + 3) % 4, (y + 2) % 4
+    own_a, own_b = set_a * 4 + y, set_b * 4 + y
+
+    def share_a(n, ys, k):
+        across(n, set_a * 4 + ys, k)
+
+    def share_b(n, ys, k):
+        @pl.when(c == 1)
+        def _():
+            across(4 + n, set_b * 4 + ys, k)
+
+    def first_hop(k):
+        arrived(own_a, k)
+        along(0, own_a, k, up)
+        arrived(own_b, k)
+        along(1, own_b, k, down)
+        along(2, own_b, k, up)
+        along(3, own_a, k, down)
+        share_a(0, y, k)
+        share_b(0, y, k)
+
+    def second_hop(k):
+        arrived(set_a * 4 + down, k)
+        along(4, set_a * 4 + down, k, up)
+        arrived(set_b * 4 + up, k)
+        along(5, set_b * 4 + up, k, down)
+        share_a(1, down, k)
+        share_b(2, up, k)
+        arrived(set_b * 4 + down, k)
+        share_b(1, down, k)
+        arrived(set_a * 4 + up, k)
+        share_a(2, up, k)
+
+    def last_hop(k):
+        arrived(set_a * 4 + far, k)
+        share_a(3, far, k)
+        arrived(set_b * 4 + far, k)
+        share_b(3, far, k)
+
+    def shared_arrived(ys):
+        @pl.when(c == 0)
+        def _():
+            for k in range(4):
+                arrived(4 + ys, k)
+                arrived(8 + ys, k)
+
+        @pl.when(c == 1)
+        def _():
+            for k in range(4):
+                arrived(ys, k)
+
+    def w_rows(t, kind):
+        return pl.ds(pl.multiple_of(kind * 1024 + t * 128, 128), 128)
+
+    def w_send(n, t, kind, to):
+        piece = wbuf.at[w_rows(t, kind)]
+        remote(piece, piece, wsend.at[n], wrecv.at[kind * 8 + t], to).start()
+
+    def w_wait(t, kind):
+        drain(wbuf.at[w_rows(t, kind)], wrecv.at[kind * 8 + t])
+
+    before, after, far_x = left * 2 + c, right * 2 + c, across_x * 2 + c
+    near_z = z + 1 - 2 * (z % 2)
+
+    def h_rows(t, half):
+        return wbuf.at[pl.ds(pl.multiple_of(1024 + t * 128 + half * 64, 64), 64)]
+
+    def h_send(n, t, to):
+        piece = h_rows(t, z % 2)
+        remote(piece, piece, hsend.at[n], hrecv.at[t, z % 2], to).start()
+
+    def h_wait(t, half):
+        drain(h_rows(t, half), hrecv.at[t, half])
+
+    def w_first():
+        out_a.wait()
+        out_c.wait()
+        h_send(0, tp, dev(z, y, right, c))
+        h_send(1, tp, dev(z, y, left, c))
+        w_send(2, tp, 0, sib)
+        w_send(3, tp, 1, sib)
+
+    def w_second():
+        h_wait(before, z % 2)
+        h_wait(after, z % 2)
+
+        @pl.when(c == 0)
+        def _():
+            h_send(2, before, dev(z, y, right, c))
+
+        @pl.when(c == 1)
+        def _():
+            h_send(2, after, dev(z, y, left, c))
+
+        w_send(0, tp, 0, dev(z, y, right, c))
+        w_send(1, tp, 0, dev(z, y, left, c))
+
+    def w_third():
+        partner = dev(near_z, y, x, c)
+        h_send(3, before, partner)
+        h_send(4, after, partner)
+
+    def w_far():
+        h_wait(far_x, z % 2)
+        h_send(5, far_x, dev(near_z, y, x, c))
+
+    def w_fourth():
+        w_wait(before, 0)
+        w_wait(after, 0)
+
+        @pl.when(c == 0)
+        def _():
+            w_send(4, before, 0, dev(z, y, right, c))
+
+        @pl.when(c == 1)
+        def _():
+            w_send(4, after, 0, dev(z, y, left, c))
+
+        w_send(5, before, 0, sib)
+        w_send(6, after, 0, sib)
+
+    def w_fifth():
+        for n, t in enumerate((before, after, far_x)):
+            h_wait(t, 1 - z % 2)
+            w_send(7 + n, t, 1, sib)
+
     def gather(n, carry):
         @pl.when(n < 4)
         def _():
-            before, after = left * 2 + c, right * 2 + c
             drain(rows(before, n), xrecv.at[before, n])
             piece = rows(before, n, 0)
             remote(piece, piece, xsend.at[2, n], xrecv.at[before, n], dev(z, y, right, c)).start()
@@ -236,6 +382,10 @@
             def _():
                 send_own(n + 2)
 
+            @pl.when(n == 3)
+            def _():
+                w_first()
+
         @pl.when(n > 0)
         def _():
             done = n - 1
@@ -248,6 +398,15 @@
                 drain(rows(t, done), xrecv.at[t, done])
             project(done)
             z_sends(done)
+            project_conv(done)
+
+        @pl.when((n > 1) & (n < 4))
+        def _():
+            first_hop(n - 2)
+
+        @pl.when(n == 3)
+        def _():
+            second_hop(n - 3)
 
         return carry
 
@@ -259,25 +418,6 @@
             gated.at[:, pl.ds(ROWS - 128, 128)], halo, hsem.at[0], hsem.at[1],
             {"sp": jnp.minimum(sp + 1, 15), "tp": tp},
         ).start()
-
-    def w_rows(t, kind):
-        return pl.ds(pl.multiple_of(kind * 1024 + t * 128, 128), 128)
-
-    def w_send(n, t, kind, to):
-        piece = wbuf.at[w_rows(t, kind)]
-        remote(piece, piece, wsend.at[n], wrecv.at[kind * 8 + t], to).start()
-
-    def w_wait(t, kind):
-        drain(wbuf.at[w_rows(t, kind)], wrecv.at[kind * 8 + t])
-
-    out_a.wait()
-    out_c.wait()
-    w_send(0, tp, 0, dev(z, y, right, c))
-    w_send(1, tp, 1, dev(z, y, left, c))
-    w_send(2, tp, 1, dev(z, y, right, c))
-    w_send(3, tp, 0, dev(z, y, left, c))
-    w_send(4, tp, 0, sib)
-    w_send(5, tp, 1, sib)
 
     def mix_conv():
         prior = jnp.concatenate([halo[...], gated[...]], axis=1).astype(F32)
@@ -291,6 +431,55 @@
             wide = jnp.concatenate([cols[5, part]] * 8, axis=1)
             cstage[part, :] = norm_rows(value[part], wide).astype(BF16)
 
+    def queries_arrived(k):
+        at = pl.ds(k * CHUNK, CHUNK)
+        for slot in range(2):
+            drain(qbuf.at[slot, pl.ds(0, QROWS), at], qrecv.at[slot, k])
+
+    def lay_keys(b, slot, lo=0, hi=ROWS):
+        block = jnp.concatenate(
+            [kvbuf[b, HEAD:, lo:hi], jnp.zeros((128 - QROWS, hi - lo), BF16)], axis=0
+        )
+        kaug[slot, lo:hi] = block.T
+
+    def fold(qs, b, s, tile, keys):
+        at = pl.ds(tile * TILE, TILE)
+        old = m_ref[qs, :, at]
+        new = jnp.maximum(old, jnp.max(s, axis=0, keepdims=True))
+        p = jnp.exp2(s - new).astype(BF16)
+        factor = jnp.exp2(old - new)
+        acc_ref[qs, :, at] = acc_ref[qs, :, at] * factor + jnp.dot(
+            kvbuf[b, 0:HEAD, 0:keys], p, preferred_element_type=F32
+        )
+        m_ref[qs, :, at] = new
+
+    def scores(slot, qs, tile, keys=ROWS):
+        return jnp.dot(
+            kaug[slot, 0:keys, :], qbuf[qs, :, pl.ds(tile * TILE, TILE)],
+            preferred_element_type=F32,
+        )
+
+    def masked(s, keys):
+        key = lax.broadcasted_iota(jnp.int32, (TILE, TILE), 0)
+        query = lax.broadcasted_iota(jnp.int32, (TILE, TILE), 1)
+        last = jnp.where(key <= query, s[keys - TILE :, :], -1e30)
+        if keys == TILE:
+            return last
+        return jnp.concatenate([s[: keys - TILE, :], last], axis=0)
+
+    def diagonal(tile):
+        keys = (tile + 1) * TILE
+        for slot, b in enumerate((own_a, own_b)):
+            lay_keys(b, slot, tile * TILE, keys)
+        for slot, b in enumerate((own_a, own_b)):
+            fold(slot, b, masked(scores(slot, slot, tile, keys), keys), tile, keys)
+
+    queries_arrived(0)
+    queries_arrived(1)
+    diagonal(0)
+    first_hop(2)
+    w_second()
+
     @pl.when(sp > 0)
     def _():
         drain(halo, hsem.at[1])
@@ -307,102 +496,20 @@
             csend.at[step], crecv.at[tp], {"sp": sp, "tp": t},
         ).start()
 
-    def arrived(b):
-        pltpu.make_async_copy(kvbuf.at[b], kvbuf.at[b], kvrecv.at[b]).wait()
-
-    def along(n, b, yy):
-        pltpu.make_async_remote_copy(
-            src_ref=kvbuf.at[b], dst_ref=kvbuf.at[b], send_sem=ysend.at[n],
-            recv_sem=kvrecv.at[b], device_id=dev(z, yy, x, c), device_id_type=MESH,
-        ).start()
-
-    def across(n, b):
-        pltpu.make_async_remote_copy(
-            src_ref=kvbuf.at[b], dst_ref=kvbuf.at[b], send_sem=dsend.at[n],
-            recv_sem=kvrecv.at[b], device_id=sib, device_id_type=MESH,
-        ).start()
-
-    up, down, far = (y + 1) % 4, (y + 3) % 4, (y + 2) % 4
-
-    def share(k, ys):
-        across(k, set_a * 4 + ys)
-
-        @pl.when(c == 1)
-        def _():
-            across(4 + k, set_b * 4 + ys)
-
-    own_a, own_b = set_a * 4 + y, set_b * 4 + y
-    arrived(own_a)
-    along(0, own_a, up)
-    across(0, own_a)
-    arrived(own_b)
-    along(1, own_b, down)
-    along(2, own_b, up)
-    along(3, own_a, down)
-
-    @pl.when(c == 1)
-    def _():
-        across(4, own_b)
-
-    for slot in range(2):
-        pltpu.make_async_copy(
-            qbuf.at[slot, pl.ds(0, QROWS)], qbuf.at[slot, pl.ds(0, QROWS)], qrecv.at[slot]
-        ).wait()
-        pltpu.make_async_copy(gbuf.at[slot], gbuf.at[slot], grecv.at[slot]).wait()
-
-    def lay_keys(b, slot):
-        block = jnp.concatenate(
-            [kvbuf[b, HEAD:, :], jnp.zeros((128 - QROWS, ROWS), BF16)], axis=0
-        )
-        kaug[slot] = block.T
-
-    def fold(qs, b, s, tile, keys):
-        at = pl.ds(tile * TILE, TILE)
-        old = m_ref[qs, :, at]
-        new = jnp.maximum(old, jnp.max(s, axis=0, keepdims=True))
-        p = jnp.exp2(s - new).astype(BF16)
-        factor = jnp.exp2(old - new)
-        acc_ref[qs, :, at] = acc_ref[qs, :, at] * factor + jnp.dot(
-            kvbuf[b, 0:HEAD, 0:keys], p, preferred_element_type=F32
-        )
-        m_ref[qs, :, at] = new
-
-    def scores(slot, qs, tile, keys=ROWS):
-        return jnp.dot(
-            kaug[slot, 0:keys, :], qbuf[qs, :, pl.ds(tile * TILE, TILE)],
-            preferred_element_type=F32,
-        )
-
-    def masked(s, keys):
-        key = lax.broadcasted_iota(jnp.int32, (TILE, TILE), 0)
-        query = lax.broadcasted_iota(jnp.int32, (TILE, TILE), 1)
-        last = jnp.where(key <= query, s[keys - TILE :, :], -1e30)
-        if keys == TILE:
-            return last
-        return jnp.concatenate([s[: keys - TILE, :], last], axis=0)
-
-    def diagonal(n, carry):
-        b = jnp.where(n == 0, own_a, own_b)
-        lay_keys(b, 0)
-        for tile in range(2):
-            keys = (tile + 1) * TILE
-            fold(n, b, masked(scores(0, n, tile, keys), keys), tile, keys)
-        return carry
-
-    lax.fori_loop(0, 2, diagonal, 0)
-
-    def group(ys, count):
-        def item(n):
-            qs = jnp.where(n < 3, jnp.where((c == 1) & (n == 0), 0, 1), n - 3)
-            always = jnp.where(c == 0, n, n // 2)
-            zs = jnp.where(n < 3, always, jnp.where(n == 3, set_a, set_b))
-            return qs, zs * 4 + ys
-
+    first_hop(3)
+    queries_arrived(2)
+    queries_arrived(3)
+    diagonal(1)
+    second_hop(1)
+    w_third()
+
+    def run(item, count, ahead):
         qs, b = item(0)
         lay_keys(b, 0)
         s_ref[0] = scores(0, qs, 0)
 
         def body(n, carry):
+            ahead(n + 1)
             qs, b = item(n)
             qn, bn = item(jnp.minimum(n + 1, count - 1))
             cur = n % 2
@@ -415,49 +522,21 @@
 
         lax.fori_loop(0, count, body, 0)
 
-    def shared_arrived(ys):
-        @pl.when(c == 0)
-        def _():
-            arrived(4 + ys)
-            arrived(8 + ys)
-
-        @pl.when(c == 1)
-        def _():
-            arrived(ys)
-
-    shared_arrived(y)
-    group(y, 3)
-    before, after, far_x = left * 2 + c, right * 2 + c, across_x * 2 + c
-
-    arrived(set_a * 4 + down)
-    along(4, set_a * 4 + down, up)
-    arrived(set_b * 4 + up)
-    along(5, set_b * 4 + up, down)
-    arrived(set_b * 4 + down)
-    share(1, down)
-    arrived(set_a * 4 + up)
-    share(2, up)
-    shared_arrived(down)
-    group(down, jnp.where(down < y, 5, 3))
-    w_wait(before, 0)
-    w_send(6, before, 0, dev(z, y, right, c))
-    w_send(7, before, 0, sib)
-    w_wait(after, 1)
-    w_send(8, after, 1, dev(z, y, left, c))
-    w_send(9, after, 1, sib)
-    arrived(set_a * 4 + far)
-    arrived(set_b * 4 + far)
-    share(3, far)
-    shared_arrived(up)
-    group(up, jnp.where(up < y, 5, 3))
-    w_wait(before, 1)
-    w_send(10, before, 1, sib)
-    w_wait(after, 0)
-    w_send(11, after, 0, sib)
-    shared_arrived(far)
-    group(far, jnp.where(far < y, 5, 3))
-
-    for slot in range(2):
+    def pick(n, ys, earlier):
+        zero = c + earlier
+        in_first = n < zero
+        first = jnp.where((c == 1) & (n == 0), 0, set_a)
+        return jnp.where(in_first, 0, 1), jnp.where(in_first, first, n - zero) * 4 + ys
+
+    def pick_near(n, ys, earlier):
+        k = n - 1 - 2 * earlier
+        shared_q = jnp.where((c == 1) & (k == 0), 0, 1)
+        shared_z = jnp.where(c == 0, 1 + k, 0)
+        qs = jnp.where(k >= 0, shared_q, jnp.where(n == 1, 0, 1))
+        zs = jnp.where(k >= 0, shared_z, jnp.where(n == 2, set_b, set_a))
+        return qs, zs * 4 + ys
+
+    def send_heads(slot):
         stage[slot] = norm_rows(acc_ref[slot], gbuf[slot][:, 0:1]).astype(BF16)
         head = x * 4 + z
         dst = cbuf.at[pl.ds(pl.multiple_of(head * HEAD, HEAD), HEAD)]
@@ -465,11 +544,9 @@
         for step in range(8):
             t = (tp + step) % 8
             piece = stage.at[slot, :, pl.ds(pl.multiple_of(t * 128, 128), 128)]
+            to = {"sp": zt * 4 + y, "tp": t}
             if step:
-                remote(
-                    piece, dst, osend.at[slot, step], arecv.at[head],
-                    {"sp": zt * 4 + y, "tp": t},
-                ).start()
+                remote(piece, dst, osend.at[slot, step], arecv.at[head], to).start()
                 continue
 
             @pl.when(zt == z)
@@ -478,15 +555,63 @@
 
             @pl.when(zt != z)
             def _():
-                remote(
-                    piece, dst, osend.at[slot, step], arecv.at[head],
-                    {"sp": zt * 4 + y, "tp": t},
-                ).start()
+                remote(piece, dst, osend.at[slot, step], arecv.at[head], to).start()
+
+    for slot in range(2):
+        drain(gbuf.at[slot], grecv.at[slot])
+    shared_arrived(y)
+    run(lambda n: pick_near(n, y, 0), 3, lambda n: None)
+    second_hop(2)
+    second_hop(3)
+    w_far()
+
+    from_down = jnp.where(down < y, 1, 0)
+    from_up = jnp.where(up < y, 1, 0)
+    from_far = jnp.where(far < y, 1, 0)
+    at_up = 3 + 2 * from_down
+    at_far = at_up + 3 + 2 * from_up
+    first_far = c + from_far
+
+    def item(n):
+        ys = jnp.where(n < at_up, down, jnp.where(n < at_far, up, far))
+        earlier = jnp.where(n < at_up, from_down, jnp.where(n < at_far, from_up, from_far))
+        start = jnp.where(n < at_up, 0, jnp.where(n < at_far, at_up, at_far))
+        late = pick(n - start, ys, earlier)
+        soon = pick_near(n - start, ys, earlier)
+        return tuple(jnp.where(n < at_far, a, b) for a, b in zip(soon, late))
+
+    def ahead(n):
+        @pl.when(n == 1 + 2 * from_down)
+        def _():
+            shared_arrived(down)
+
+        @pl.when(n == 2)
+        def _():
+            last_hop(0)
+            last_hop(1)
+
+        @pl.when(n == jnp.minimum(8, at_far + first_far))
+        def _():
+            w_fourth()
+
+        @pl.when(n == at_up)
+        def _():
+            last_hop(2)
+            last_hop(3)
+            shared_arrived(up)
+
+        @pl.when(n == at_far)
+        def _():
+            shared_arrived(far)
+
+    run(item, at_far + first_far, ahead)
+    send_heads(0)
+    w_fifth()
+    run(lambda n: pick(n + first_far, far, from_far), 3 - c + from_far, lambda n: None)
+    send_heads(1)
 
     w_wait(far_x, 0)
-    w_send(12, far_x, 0, sib)
-    w_wait(far_x, 1)
-    w_send(13, far_x, 1, sib)
+    w_send(10, far_x, 0, sib)
     for xx in range(4):
         w_wait(xx * 2 + 1 - c, 0)
         w_wait(xx * 2 + 1 - c, 1)
@@ -494,25 +619,29 @@
         drain(cbuf.at[pl.ds(1024 + t * 128, 128)], crecv.at[t])
 
     def product(lo, n):
-        at = pl.ds(pl.multiple_of(n * TILE, TILE), TILE)
+        at = pl.ds(n * TILE, TILE)
         return jnp.dot(
-            cbuf[lo : lo + 1024, :].T, wbuf[lo : lo + 1024, at], preferred_element_type=F32
+            ct[:, lo : lo + 1024], wbuf[lo : lo + 1024, at], preferred_element_type=F32
         )
 
     def conv_part(n, carry):
-        oacc[:, pl.ds(pl.multiple_of(n * TILE, TILE), TILE)] = product(1024, n)
+        oacc[:, pl.ds(n * TILE, TILE)] = product(1024, n)
         return carry
 
-    lax.fori_loop(0, WIDTH // TILE, conv_part, 0)
+    ct[:, 1024:] = cbuf[1024:, :].T
+    for n in range(WIDTH // TILE):
+        conv_part(n, 0)
     for h in range(16):
         drain(cbuf.at[pl.ds(h * HEAD, HEAD)], arecv.at[h])
 
     def attn_part(n, carry):
-        at = pl.ds(pl.multiple_of(n * TILE, TILE), TILE)
+        at = pl.ds(n * TILE, TILE)
         out_ref[:, at] = (oacc[:, at] + product(0, n)).astype(BF16)
         return carry
 
-    lax.fori_loop(0, WIDTH // TILE, attn_part, 0)
+    ct[:, :1024] = cbuf[:1024, :].T
+    for n in range(WIDTH // TILE):
+        attn_part(n, 0)
 
     def sent(n, carry):
         for k in range(2):
@@ -530,6 +659,16 @@
                 drain(kvout.at[i, :, at], zsend.at[i, 0, n])
                 drain(qout.at[i, :, at], zsend.at[i, 1, n])
 
+        for k in range(6):
+            drain(chunk(0, n), ysend.at[k, n])
+        for k in range(4):
+            drain(chunk(0, n), dsend.at[k, n])
+
+        @pl.when(c == 1)
+        def _():
+            for k in range(4, 8):
+                drain(chunk(0, n), dsend.at[k, n])
+
         return carry
 
     lax.fori_loop(0, 4, sent, 0)
@@ -545,18 +684,10 @@
     def _():
         drain(halo, hsem.at[0])
 
+    for n in range(11):
+        drain(wbuf.at[pl.ds(0, 128)], wsend.at[n])
     for n in range(6):
-        drain(kvbuf.at[0], ysend.at[n])
-    for n in range(4):
-        drain(kvbuf.at[0], dsend.at[n])
-
-    @pl.when(c == 1)
-    def _():
-        for n in range(4, 8):
-            drain(kvbuf.at[0], dsend.at[n])
-
-    for n in range(14):
-        drain(wbuf.at[pl.ds(0, 128)], wsend.at[n])
+        drain(wbuf.at[pl.ds(0, 64)], hsend.at[n])
     for step in range(1, 8):
         drain(cbuf.at[pl.ds(0, 128)], csend.at[step])
     for slot in range(2):
@@ -568,6 +699,12 @@
         @pl.when(zt != z)
         def _():
             drain(piece, osend.at[slot, 0])
+
+
+def store_kernel(rows, out, sem):
+    copy = pltpu.make_async_copy(rows, out, sem)
+    copy.start()
+    copy.wait()
 
 
 def per_device(
@@ -578,9 +715,9 @@
     DMA = pltpu.SemaphoreType.DMA
     far = pl.BlockSpec(memory_space=pl.ANY)
     near = pl.BlockSpec(memory_space=VMEM)
-    return pl.pallas_call(
+    rows = pl.pallas_call(
         layer_kernel,
-        out_shape=jax.ShapeDtypeStruct((128, WIDTH), BF16),
+        out_shape=pltpu.VMEM((128, WIDTH), BF16),
         in_specs=[far, near] + [far] * 6 + [near] * 6 + [far] * 2,
         out_specs=near,
         scratch_shapes=[
@@ -588,6 +725,7 @@
             VMEM((6, WIDTH, 128), BF16),
             VMEM((768, WIDTH), BF16),
             VMEM((CHUNK, WIDTH), BF16),
+            VMEM((1, CHUNK), F32),
             VMEM((768, CHUNK), F32),
             VMEM((128, ROWS), F32),
             VMEM((128, ROWS), BF16),
@@ -607,10 +745,11 @@
             VMEM((128, ROWS), BF16),
             VMEM((WIDTH, WIDTH), BF16),
             VMEM((WIDTH, 128), BF16),
+            VMEM((128, WIDTH), BF16),
             VMEM((128, WIDTH), F32),
             DMA((9,)), DMA((4, 4)), DMA((4, 4)), DMA((8, 4)), DMA((2,)),
-            DMA((2, 2, 4)), DMA((2,)), DMA((6,)), DMA((8,)), DMA((2, 8)), DMA((8,)), DMA((14,)),
-            DMA((2,)), DMA((16,)), DMA((2,)), DMA((16,)), DMA((16,)), DMA((8,)),
+            DMA((2, 2, 4)), DMA((2,)), DMA((6, 4)), DMA((8, 4)), DMA((2, 8)), DMA((8,)), DMA((11,)), DMA((6,)),
+            DMA((2, 4)), DMA((16, 4)), DMA((2,)), DMA((16,)), DMA((8, 2)), DMA((16,)), DMA((8,)),
         ],
         compiler_params=pltpu.CompilerParams(
             collective_id=1, has_side_effects=True, vmem_limit_bytes=56 * 2**20
@@ -622,6 +761,14 @@
         key_gain.reshape(1, HEAD), gate_totals.T, conv_taps, attn_out_gain.reshape(1, 128),
         conv_out_gain.reshape(1, 128), attn_out_weight, conv_out_weight,
     )
+    return pl.pallas_call(
+        store_kernel,
+        out_shape=jax.ShapeDtypeStruct((128, WIDTH), BF16),
+        in_specs=[near],
+        out_specs=far,
+        scratch_shapes=[DMA],
+        name="store",
+    )(pltpu.with_memory_space_constraint(rows, pltpu.VMEM))
 
 
 def solution(mesh):

time: 81.9 us -> 72.5 us (0.89)
  Pallas kernels: 79.8 us -> 72.3 us
  local copies, waits for them, and re-layouts: 1.88 us -> 0 us
    pallas_call x1 -> x2, Pallas kernels: 79.8 us -> 72.3 us  [the longest x1 71.5 us: per_device(): pl.pallas_call(layer_kernel, out_shape=pltpu.VMEM((128, WIDTH), BF16), in...]
    unnamed x1 -> x0, local copies, waits for them, and re-layouts: 1.88 us -> none
where the time goes in v3:
time: 72.5 us; the launch traced here: 72.3 us
  Pallas kernels  72.3 us (100%)
    pallas_call x1, Pallas kernels, per_device(): pl.pallas_call(layer_kernel, out_shape=pltpu.VMEM((128, WIDTH), BF16), in...  71.5 us

profile of v3, /device:TPU:1, one launch (start us, length us, event | category | flops | bytes accessed | tf_op | source)
XLA Modules:
  0.0 72.3 jit_solution(8159865068687294971)
XLA Ops:
  0.0 71.5 %layer.1.rows = bf16[128,2048]{1,0:T(8,128)(2,1)S(1)} custom-call(bf16[1024,256]{1,0:T(8,128)(2,1)} %tokens.1, f32[1,2048]{1,0:T(1,128)} %bitcast.6, bf16[2048,128]{1,0:T(8,128)(2,1)} %wq.1, bf16[2048,128]{1,0:T(8,128)(2,1)} %wk.1, bf16[2048,128]{1,0:T(8,128)(2,1)} %wv.1, bf16[2048,128]{1,0:T(8,128)(2,1)} %wo.1, bf16[2048,128]{1,0:T(8,128)(2,1)} %wi.1, ...), custom_call_target="tpu_custom_call" | custom-call | tf_op jit(solution)/shard_map/layer/pallas_call | solution.py:718
  71.5 0.8 %store.1 = bf16[128,2048]{1,0:T(8,128)(2,1)} custom-call(bf16[128,2048]{1,0:T(8,128)(2,1)S(1)} %layer.1.rows), custom_call_target="tpu_custom_call" | custom-call | tf_op jit(solution)/shard_map/store/pallas_call | solution.py:764

commit v4 on v3

--- a/solution.py
+++ b/solution.py
@@ -33,8 +33,8 @@
 
 
 def layer_kernel(
-    tokens, mix, wq, wk, wv, wo, wi, wx, qgain, kgain, gates, taps, again, cgain, wa, wc,
-    out_ref,
+    tokens, mix_in, wq, wk, wv, wo, wi, wx, qgain_in, kgain_in, gates_in, taps_in, again_in,
+    cgain_in, wa, wc, out_ref, mix, qgain, kgain, gates, taps, again, cgain,
     xbuf, wtmp, wt, xs, scale_ref, proj, outer, gated, halo, qout, kvout, gout, cols,
     qbuf, kvbuf, gbuf, kaug, s_ref, m_ref, acc_ref, stage, cstage, wbuf, cbuf, ct, oacc,
     lsem, xsend, xdsend, xrecv, hsem, zsend, gsend, ysend, dsend, osend, csend, wsend, hsend,
@@ -68,15 +68,24 @@
     weights = [
         local(w, wtmp.at[n], lsem.at[1 + n]) for n, w in enumerate((wq, wk, wv, wo, wi, wx))
     ]
-    for w in weights:
-        w.start()
     own_wa = pl.ds(pl.multiple_of(tp * 128, 128), 128)
     own_wc = pl.ds(pl.multiple_of(1024 + tp * 128, 128), 128)
     out_a = local(wa, wbuf.at[own_wa], lsem.at[7])
     out_c = local(wc, wbuf.at[own_wc], lsem.at[8])
+    smalls = [
+        local(src, dst, lsem.at[9 + n])
+        for n, (src, dst) in enumerate((
+            (qgain_in, qgain), (kgain_in, kgain), (gates_in, gates), (taps_in, taps),
+            (again_in, again), (cgain_in, cgain), (mix_in, mix),
+        ))
+    ]
+    for small in smalls:
+        small.start()
+
+    for w in weights:
+        w.start()
     out_a.start()
     out_c.start()
-
     barrier = pltpu.get_barrier_semaphore()
 
     def greet(step, carry):
@@ -116,6 +125,8 @@
     send_own(0)
     send_own(1)
 
+    for small in smalls:
+        small.wait()
     for n, row in enumerate((qgain, kgain)):
         both = jnp.concatenate([row[...], row[...]], axis=1)
         if n == 0:
@@ -198,12 +209,12 @@
             piece = xbuf[t, at, :].astype(F32)
             squares = squares + piece[:, :128] * piece[:, :128] + piece[:, 128:] * piece[:, 128:]
             lanes = slice(t * FEATURES, (t + 1) * FEATURES)
-            xs[:, lanes] = (piece * mix[:, lanes]).astype(BF16)
+            xs[n, :, lanes] = (piece * mix[:, lanes]).astype(BF16)
         total = jnp.sum(squares.T, axis=0, keepdims=True)
         row_scale = lax.rsqrt(total / WIDTH + NORM_EPSILON)
-        scale_ref[...] = row_scale
+        scale_ref[n] = row_scale
         proj[0:384] = lax.dot_general(
-            wt[0:384], xs[...], (((1,), (1,)), ((), ())), preferred_element_type=F32
+            wt[0:384], xs[n], (((1,), (1,)), ((), ())), preferred_element_type=F32
         ) * row_scale
         for i in range(2):
             lo = i * HEAD
@@ -219,8 +230,8 @@
     def project_conv(n):
         at = pl.ds(pl.multiple_of(n * CHUNK, CHUNK), CHUNK)
         proj[384:768] = lax.dot_general(
-            wt[384:768], xs[...], (((1,), (1,)), ((), ())), preferred_element_type=F32
-        ) * scale_ref[...]
+            wt[384:768], xs[n], (((1,), (1,)), ((), ())), preferred_element_type=F32
+        ) * scale_ref[n]
         outer[:, at] = proj[384:512]
         gated[:, at] = (proj[512:640] * proj[640:768]).astype(BF16)
 
@@ -398,7 +409,6 @@
                 drain(rows(t, done), xrecv.at[t, done])
             project(done)
             z_sends(done)
-            project_conv(done)
 
         @pl.when((n > 1) & (n < 4))
         def _():
@@ -411,6 +421,7 @@
         return carry
 
     lax.fori_loop(0, 5, gather, 0)
+    project_conv(3)
 
     @pl.when(sp < 15)
     def _():
@@ -480,6 +491,18 @@
     first_hop(2)
     w_second()
 
+    def conv_rest(n, carry):
+        project_conv(n)
+        return carry
+
+    lax.fori_loop(0, 3, conv_rest, 0)
+    first_hop(3)
+    queries_arrived(2)
+    queries_arrived(3)
+    diagonal(1)
+    second_hop(1)
+    w_third()
+
     @pl.when(sp > 0)
     def _():
         drain(halo, hsem.at[1])
@@ -496,12 +519,6 @@
             csend.at[step], crecv.at[tp], {"sp": sp, "tp": t},
         ).start()
 
-    first_hop(3)
-    queries_arrived(2)
-    queries_arrived(3)
-    diagonal(1)
-    second_hop(1)
-    w_third()
 
     def run(item, count, ahead):
         qs, b = item(0)
@@ -606,9 +623,9 @@
 
     run(item, at_far + first_far, ahead)
     send_heads(0)
-    w_fifth()
     run(lambda n: pick(n + first_far, far, from_far), 3 - c + from_far, lambda n: None)
     send_heads(1)
+    w_fifth()
 
     w_wait(far_x, 0)
     w_send(10, far_x, 0, sib)
@@ -718,14 +735,21 @@
     rows = pl.pallas_call(
         layer_kernel,
         out_shape=pltpu.VMEM((128, WIDTH), BF16),
-        in_specs=[far, near] + [far] * 6 + [near] * 6 + [far] * 2,
+        in_specs=[far] * 16,
         out_specs=near,
         scratch_shapes=[
+            VMEM((1, WIDTH), F32),
+            VMEM((1, HEAD), F32),
+            VMEM((1, HEAD), F32),
+            VMEM((2, ROWS), F32),
+            VMEM((3, 128), F32),
+            VMEM((1, 128), F32),
+            VMEM((1, 128), F32),
             VMEM((8, ROWS, FEATURES), BF16),
             VMEM((6, WIDTH, 128), BF16),
             VMEM((768, WIDTH), BF16),
-            VMEM((CHUNK, WIDTH), BF16),
-            VMEM((1, CHUNK), F32),
+            VMEM((4, CHUNK, WIDTH), BF16),
+            VMEM((4, 1, CHUNK), F32),
             VMEM((768, CHUNK), F32),
             VMEM((128, ROWS), F32),
             VMEM((128, ROWS), BF16),
@@ -747,7 +771,7 @@
             VMEM((WIDTH, 128), BF16),
             VMEM((128, WIDTH), BF16),
             VMEM((128, WIDTH), F32),
-            DMA((9,)), DMA((4, 4)), DMA((4, 4)), DMA((8, 4)), DMA((2,)),
+            DMA((16,)), DMA((4, 4)), DMA((4, 4)), DMA((8, 4)), DMA((2,)),
             DMA((2, 2, 4)), DMA((2,)), DMA((6, 4)), DMA((8, 4)), DMA((2, 8)), DMA((8,)), DMA((11,)), DMA((6,)),
             DMA((2, 4)), DMA((16, 4)), DMA((2,)), DMA((16,)), DMA((8, 2)), DMA((16,)), DMA((8,)),
         ],

time: 72.5 us -> 71.4 us (0.985)
  Pallas kernels: 72.3 us -> 71 us
    pallas_call x1, Pallas kernels: 71.5 us -> 70.2 us  [per_device(): pl.pallas_call(layer_kernel, out_shape=pltpu.VMEM((128, WIDTH), BF16), in...]
where the time goes in v4:
time: 71.4 us; the launch traced here: 71 us
  Pallas kernels  71 us (99%)
    pallas_call x1, Pallas kernels, per_device(): pl.pallas_call(layer_kernel, out_shape=pltpu.VMEM((128, WIDTH), BF16), in...  70.2 us

profile of v4, /device:TPU:1, one launch (start us, length us, event | category | flops | bytes accessed | tf_op | source)
XLA Modules:
  0.0 71.0 jit_solution(10062355219429019225)
XLA Ops:
  0.0 70.2 %layer.1.rows = bf16[128,2048]{1,0:T(8,128)(2,1)S(1)} custom-call(bf16[1024,256]{1,0:T(8,128)(2,1)} %tokens.1, f32[1,2048]{1,0:T(1,128)} %bitcast.6, bf16[2048,128]{1,0:T(8,128)(2,1)} %wq.1, bf16[2048,128]{1,0:T(8,128)(2,1)} %wk.1, bf16[2048,128]{1,0:T(8,128)(2,1)} %wv.1, bf16[2048,128]{1,0:T(8,128)(2,1)} %wo.1, bf16[2048,128]{1,0:T(8,128)(2,1)} %wi.1, ...), custom_call_target="tpu_custom_call" | custom-call | tf_op jit(solution)/shard_map/layer/pallas_call | solution.py:735
  70.2 0.8 %store.1 = bf16[128,2048]{1,0:T(8,128)(2,1)} custom-call(bf16[128,2048]{1,0:T(8,128)(2,1)S(1)} %layer.1.rows), custom_call_target="tpu_custom_call" | custom-call | tf_op jit(solution)/shard_map/store/pallas_call | solution.py:788

commit v5 on v4

--- a/solution.py
+++ b/solution.py
@@ -37,8 +37,8 @@
     cgain_in, wa, wc, out_ref, mix, qgain, kgain, gates, taps, again, cgain,
     xbuf, wtmp, wt, xs, scale_ref, proj, outer, gated, halo, qout, kvout, gout, cols,
     qbuf, kvbuf, gbuf, kaug, s_ref, m_ref, acc_ref, stage, cstage, wbuf, cbuf, ct, oacc,
-    lsem, xsend, xdsend, xrecv, hsem, zsend, gsend, ysend, dsend, osend, csend, wsend, hsend,
-    qrecv, kvrecv, grecv, wrecv, hrecv, arecv, crecv,
+    lsem, xsend, xdsend, xrecv, xshare, hsem, zsend, gsend, ysend, dsend, osend, csend, wsend,
+    hsend, hdsend, qrecv, kvrecv, kvshare, grecv, wrecv, wshare, hrecv, hshare, arecv, crecv,
 ):
     sp = lax.axis_index("sp")
     tp = lax.axis_index("tp")
@@ -118,9 +118,9 @@
 
     def send_own(n):
         piece = rows(tp, n)
-        remote(piece, piece, xsend.at[0, n], xrecv.at[tp, n], dev(z, y, right, c)).start()
-        remote(piece, piece, xsend.at[1, n], xrecv.at[tp, n], dev(z, y, left, c)).start()
-        remote(piece, piece, xdsend.at[0, n], xrecv.at[tp, n], sib).start()
+        remote(piece, piece, xsend.at[0], xrecv.at[tp // 2, n], dev(z, y, right, c)).start()
+        remote(piece, piece, xsend.at[0], xrecv.at[tp // 2, n], dev(z, y, left, c)).start()
+        remote(piece, piece, xdsend.at[0], xshare.at[n], sib).start()
 
     send_own(0)
     send_own(1)
@@ -168,13 +168,16 @@
 
     qslot = z // 2
 
+    def native(b):
+        return jnp.where(b < 8, 0, 4) + b % 4
+
     def z_sends(n):
         at = pl.ds(pl.multiple_of(n * CHUNK, CHUNK), CHUNK)
         for i in range(2):
             zt = 2 * c + i
             own = (zt == z) & (zc == c)
             pieces = (
-                (kvout.at[i, :, at], kvbuf.at[sp, :, at], kvrecv.at[sp, n]),
+                (kvout.at[i, :, at], kvbuf.at[sp, :, at], kvrecv.at[native(sp), n]),
                 (qout.at[i, :, at], qbuf.at[qslot, pl.ds(0, QROWS), at], qrecv.at[qslot, n]),
             )
 
@@ -186,7 +189,7 @@
             @pl.when(jnp.logical_not(own))
             def _():
                 for k, (src, dst, recv) in enumerate(pieces):
-                    remote(src, dst, zsend.at[i, k, n], recv, dev(zt, y, x, zc)).start()
+                    remote(src, dst, zsend.at[i, k], recv, dev(zt, y, x, zc)).start()
 
     for i in range(2):
         zt = 2 * c + i
@@ -239,15 +242,15 @@
         return kvbuf.at[b, :, pl.ds(pl.multiple_of(k * CHUNK, CHUNK), CHUNK)]
 
     def arrived(b, k):
-        drain(chunk(b, k), kvrecv.at[b, k])
+        drain(chunk(b, k), kvrecv.at[native(b), k])
 
     def along(n, b, k, yy):
         piece = chunk(b, k)
-        remote(piece, piece, ysend.at[n, k], kvrecv.at[b, k], dev(z, yy, x, c)).start()
+        remote(piece, piece, ysend.at[0], kvrecv.at[native(b), k], dev(z, yy, x, c)).start()
 
     def across(n, b, k):
         piece = chunk(b, k)
-        remote(piece, piece, dsend.at[n, k], kvrecv.at[b, k], sib).start()
+        remote(piece, piece, dsend.at[n // 4], kvshare.at[b % 4], sib).start()
 
     up, down, far = (y + 1) % 4, (y + 3) % 4, (y + 2) % 4
     own_a, own_b = set_a * 4 + y, set_b * 4 + y
@@ -291,24 +294,25 @@
     def shared_arrived(ys):
         @pl.when(c == 0)
         def _():
-            for k in range(4):
-                arrived(4 + ys, k)
-                arrived(8 + ys, k)
+            drain(kvbuf.at[pl.ds(0, 2)], kvshare.at[ys])
 
         @pl.when(c == 1)
         def _():
-            for k in range(4):
-                arrived(ys, k)
+            drain(kvbuf.at[0], kvshare.at[ys])
 
     def w_rows(t, kind):
         return pl.ds(pl.multiple_of(kind * 1024 + t * 128, 128), 128)
 
     def w_send(n, t, kind, to):
         piece = wbuf.at[w_rows(t, kind)]
-        remote(piece, piece, wsend.at[n], wrecv.at[kind * 8 + t], to).start()
+        remote(piece, piece, wsend.at[0], wrecv.at[t // 2], to).start()
+
+    def w_across(t):
+        piece = wbuf.at[w_rows(t, 0)]
+        remote(piece, piece, wsend.at[0], wshare.at[0], sib).start()
 
     def w_wait(t, kind):
-        drain(wbuf.at[w_rows(t, kind)], wrecv.at[kind * 8 + t])
+        drain(wbuf.at[w_rows(t, kind)], wrecv.at[t // 2])
 
     before, after, far_x = left * 2 + c, right * 2 + c, across_x * 2 + c
     near_z = z + 1 - 2 * (z % 2)
@@ -318,18 +322,23 @@
 
     def h_send(n, t, to):
         piece = h_rows(t, z % 2)
-        remote(piece, piece, hsend.at[n], hrecv.at[t, z % 2], to).start()
+        remote(piece, piece, hsend.at[0], hrecv.at[t // 2, z % 2], to).start()
+
+    def h_across(n, t, half):
+        piece = h_rows(t, half)
+        remote(piece, piece, hdsend.at[0], hshare.at[0], sib).start()
 
     def h_wait(t, half):
-        drain(h_rows(t, half), hrecv.at[t, half])
+        drain(h_rows(t, half), hrecv.at[t // 2, half])
 
     def w_first():
         out_a.wait()
         out_c.wait()
         h_send(0, tp, dev(z, y, right, c))
         h_send(1, tp, dev(z, y, left, c))
-        w_send(2, tp, 0, sib)
-        w_send(3, tp, 1, sib)
+        w_across(tp)
+        h_across(0, tp, 0)
+        h_across(1, tp, 1)
 
     def w_second():
         h_wait(before, z % 2)
@@ -350,10 +359,13 @@
         partner = dev(near_z, y, x, c)
         h_send(3, before, partner)
         h_send(4, after, partner)
+        h_across(2, before, z % 2)
+        h_across(3, after, z % 2)
 
     def w_far():
         h_wait(far_x, z % 2)
         h_send(5, far_x, dev(near_z, y, x, c))
+        h_across(4, far_x, z % 2)
 
     def w_fourth():
         w_wait(before, 0)
@@ -367,27 +379,27 @@
         def _():
             w_send(4, after, 0, dev(z, y, left, c))
 
-        w_send(5, before, 0, sib)
-        w_send(6, after, 0, sib)
+        w_across(before)
+        w_across(after)
 
     def w_fifth():
         for n, t in enumerate((before, after, far_x)):
             h_wait(t, 1 - z % 2)
-            w_send(7 + n, t, 1, sib)
+            h_across(5 + n, t, 1 - z % 2)
 
     def gather(n, carry):
         @pl.when(n < 4)
         def _():
-            drain(rows(before, n), xrecv.at[before, n])
+            drain(rows(before, n), xrecv.at[before // 2, n])
             piece = rows(before, n, 0)
-            remote(piece, piece, xsend.at[2, n], xrecv.at[before, n], dev(z, y, right, c)).start()
+            remote(piece, piece, xsend.at[0], xrecv.at[before // 2, n], dev(z, y, right, c)).start()
             piece = rows(before, n)
-            remote(piece, piece, xdsend.at[1, n], xrecv.at[before, n], sib).start()
-            drain(rows(after, n), xrecv.at[after, n])
+            remote(piece, piece, xdsend.at[0], xshare.at[n], sib).start()
+            drain(rows(after, n), xrecv.at[after // 2, n])
             piece = rows(after, n, 1)
-            remote(piece, piece, xsend.at[3, n], xrecv.at[after, n], dev(z, y, left, c)).start()
+            remote(piece, piece, xsend.at[0], xrecv.at[after // 2, n], dev(z, y, left, c)).start()
             piece = rows(after, n)
-            remote(piece, piece, xdsend.at[2, n], xrecv.at[after, n], sib).start()
+            remote(piece, piece, xdsend.at[0], xshare.at[n], sib).start()
 
             @pl.when(n < 2)
             def _():
@@ -397,30 +409,28 @@
             def _():
                 w_first()
 
+        @pl.when(n > 2)
+        def _():
+            first_hop(n - 3)
+
         @pl.when(n > 0)
         def _():
             done = n - 1
             far = across_x * 2 + c
-            drain(rows(far, done), xrecv.at[far, done])
+            drain(rows(far, done), xrecv.at[far // 2, done])
             piece = rows(far, done)
-            remote(piece, piece, xdsend.at[3, done], xrecv.at[far, done], sib).start()
-            for xx in range(4):
-                t = xx * 2 + 1 - c
-                drain(rows(t, done), xrecv.at[t, done])
+            remote(piece, piece, xdsend.at[0], xshare.at[done], sib).start()
+            drain(
+                xbuf.at[pl.ds(0, 4), pl.ds(pl.multiple_of(done * CHUNK, CHUNK), CHUNK)],
+                xshare.at[done],
+            )
             project(done)
             z_sends(done)
 
-        @pl.when((n > 1) & (n < 4))
-        def _():
-            first_hop(n - 2)
-
-        @pl.when(n == 3)
-        def _():
-            second_hop(n - 3)
-
         return carry
 
     lax.fori_loop(0, 5, gather, 0)
+    second_hop(0)
     project_conv(3)
 
     @pl.when(sp < 15)
@@ -510,13 +520,13 @@
     mix_conv()
     to_rows = pl.ds(pl.multiple_of(1024 + tp * 128, 128), 128)
     local(
-        cstage.at[:, pl.ds(pl.multiple_of(tp * 128, 128), 128)], cbuf.at[to_rows], crecv.at[tp]
+        cstage.at[:, pl.ds(pl.multiple_of(tp * 128, 128), 128)], cbuf.at[to_rows], crecv.at[0]
     ).start()
     for step in range(1, 8):
         t = (tp + step) % 8
         remote(
             cstage.at[:, pl.ds(pl.multiple_of(t * 128, 128), 128)], cbuf.at[to_rows],
-            csend.at[step], crecv.at[tp], {"sp": sp, "tp": t},
+            csend.at[0], crecv.at[0], {"sp": sp, "tp": t},
         ).start()
 
 
@@ -539,11 +549,13 @@
 
         lax.fori_loop(0, count, body, 0)
 
-    def pick(n, ys, earlier):
-        zero = c + earlier
-        in_first = n < zero
-        first = jnp.where((c == 1) & (n == 0), 0, set_a)
-        return jnp.where(in_first, 0, 1), jnp.where(in_first, first, n - zero) * 4 + ys
+    def pick_far(n, ys, earlier):
+        early = jnp.where(c == 0, earlier, 2 + earlier)
+        k = n - early
+        early_z = jnp.where(c == 0, set_a, n)
+        late_z = jnp.where(c == 0, k, jnp.where(k == 0, 0, set_a))
+        qs = jnp.where(k < 0, c, 1 - c)
+        return qs, jnp.where(k < 0, early_z, late_z) * 4 + ys
 
     def pick_near(n, ys, earlier):
         k = n - 1 - 2 * earlier
@@ -563,16 +575,16 @@
             piece = stage.at[slot, :, pl.ds(pl.multiple_of(t * 128, 128), 128)]
             to = {"sp": zt * 4 + y, "tp": t}
             if step:
-                remote(piece, dst, osend.at[slot, step], arecv.at[head], to).start()
+                remote(piece, dst, osend.at[slot], arecv.at[0], to).start()
                 continue
 
             @pl.when(zt == z)
             def _():
-                local(piece, dst, arecv.at[head]).start()
+                local(piece, dst, arecv.at[0]).start()
 
             @pl.when(zt != z)
             def _():
-                remote(piece, dst, osend.at[slot, step], arecv.at[head], to).start()
+                remote(piece, dst, osend.at[2 + slot], arecv.at[0], to).start()
 
     for slot in range(2):
         drain(gbuf.at[slot], grecv.at[slot])
@@ -587,13 +599,14 @@
     from_far = jnp.where(far < y, 1, 0)
     at_up = 3 + 2 * from_down
     at_far = at_up + 3 + 2 * from_up
-    first_far = c + from_far
+    first_far = jnp.where(c == 0, from_far, 2 + from_far)
+    last_item = at_far + 2 + 2 * from_far
 
     def item(n):
         ys = jnp.where(n < at_up, down, jnp.where(n < at_far, up, far))
         earlier = jnp.where(n < at_up, from_down, jnp.where(n < at_far, from_up, from_far))
         start = jnp.where(n < at_up, 0, jnp.where(n < at_far, at_up, at_far))
-        late = pick(n - start, ys, earlier)
+        late = pick_far(n - at_far, far, from_far)
         soon = pick_near(n - start, ys, earlier)
         return tuple(jnp.where(n < at_far, a, b) for a, b in zip(soon, late))
 
@@ -607,7 +620,15 @@
             last_hop(0)
             last_hop(1)
 
-        @pl.when(n == jnp.minimum(8, at_far + first_far))
+        @pl.when((n == last_item) & (y > 1))
+        def _():
+            w_fifth()
+
+        @pl.when(n == at_far + first_far + 1)
+        def _():
+            send_heads(c)
+
+        @pl.when(n == jnp.where(y == 0, 5, 7))
         def _():
             w_fourth()
 
@@ -621,19 +642,17 @@
         def _():
             shared_arrived(far)
 
-    run(item, at_far + first_far, ahead)
-    send_heads(0)
-    run(lambda n: pick(n + first_far, far, from_far), 3 - c + from_far, lambda n: None)
-    send_heads(1)
-    w_fifth()
+    run(item, at_far + 3 + 2 * from_far, ahead)
+    send_heads(1 - c)
+
+    @pl.when(y < 2)
+    def _():
+        w_fifth()
 
     w_wait(far_x, 0)
-    w_send(10, far_x, 0, sib)
-    for xx in range(4):
-        w_wait(xx * 2 + 1 - c, 0)
-        w_wait(xx * 2 + 1 - c, 1)
-    for t in range(8):
-        drain(cbuf.at[pl.ds(1024 + t * 128, 128)], crecv.at[t])
+    w_across(far_x)
+    drain(wbuf.at[pl.ds(0, 512)], hshare.at[0])
+    drain(cbuf.at[pl.ds(1024, 1024)], crecv.at[0])
 
     def product(lo, n):
         at = pl.ds(n * TILE, TILE)
@@ -648,8 +667,8 @@
     ct[:, 1024:] = cbuf[1024:, :].T
     for n in range(WIDTH // TILE):
         conv_part(n, 0)
-    for h in range(16):
-        drain(cbuf.at[pl.ds(h * HEAD, HEAD)], arecv.at[h])
+    drain(wbuf.at[pl.ds(0, 512)], wshare.at[0])
+    drain(cbuf.at[pl.ds(0, 1024)], arecv.at[0])
 
     def attn_part(n, carry):
         at = pl.ds(n * TILE, TILE)
@@ -660,35 +679,15 @@
     for n in range(WIDTH // TILE):
         attn_part(n, 0)
 
-    def sent(n, carry):
-        for k in range(2):
-            drain(rows(tp, n), xsend.at[k, n])
-            drain(rows(tp, n, 0), xsend.at[2 + k, n])
-        for k in range(4):
-            drain(rows(tp, n), xdsend.at[k, n])
-        for i in range(2):
-            zt = 2 * c + i
-            own = (zt == z) & (zc == c)
-            at = pl.ds(pl.multiple_of(n * CHUNK, CHUNK), CHUNK)
-
-            @pl.when(jnp.logical_not(own))
-            def _():
-                drain(kvout.at[i, :, at], zsend.at[i, 0, n])
-                drain(qout.at[i, :, at], zsend.at[i, 1, n])
-
-        for k in range(6):
-            drain(chunk(0, n), ysend.at[k, n])
-        for k in range(4):
-            drain(chunk(0, n), dsend.at[k, n])
-
-        @pl.when(c == 1)
-        def _():
-            for k in range(4, 8):
-                drain(chunk(0, n), dsend.at[k, n])
-
-        return carry
-
-    lax.fori_loop(0, 4, sent, 0)
+    drain(xbuf.at[pl.ds(0, 3)], xsend.at[0])
+    drain(xbuf.at[pl.ds(0, 4)], xdsend.at[0])
+    drain(kvbuf.at[pl.ds(0, 6)], ysend.at[0])
+    drain(kvbuf.at[pl.ds(0, 4)], dsend.at[0])
+
+    @pl.when(c == 1)
+    def _():
+        drain(kvbuf.at[pl.ds(0, 4)], dsend.at[1])
+
     for i in range(2):
         zt = 2 * c + i
         own = (zt == z) & (zc == c)
@@ -696,26 +695,24 @@
         @pl.when(jnp.logical_not(own))
         def _():
             drain(gout.at[i], gsend.at[i])
+            drain(kvout.at[i], zsend.at[i, 0])
+            drain(qout.at[i], zsend.at[i, 1])
 
     @pl.when(sp < 15)
     def _():
         drain(halo, hsem.at[0])
 
-    for n in range(11):
-        drain(wbuf.at[pl.ds(0, 128)], wsend.at[n])
-    for n in range(6):
-        drain(wbuf.at[pl.ds(0, 64)], hsend.at[n])
-    for step in range(1, 8):
-        drain(cbuf.at[pl.ds(0, 128)], csend.at[step])
+    drain(wbuf.at[pl.ds(0, 896)], wsend.at[0])
+    drain(wbuf.at[pl.ds(0, 512)], hdsend.at[0])
+    drain(wbuf.at[pl.ds(0, 384)], hsend.at[0])
+    drain(cbuf.at[pl.ds(0, 896)], csend.at[0])
     for slot in range(2):
         zt = jnp.where(slot == 0, set_a, set_b)
-        piece = stage.at[slot, :, pl.ds(0, 128)]
-        for step in range(1, 8):
-            drain(piece, osend.at[slot, step])
+        drain(stage.at[slot, :, pl.ds(0, 896)], osend.at[slot])
 
         @pl.when(zt != z)
         def _():
-            drain(piece, osend.at[slot, 0])
+            drain(stage.at[slot, :, pl.ds(0, 128)], osend.at[2 + slot])
 
 
 def store_kernel(rows, out, sem):
@@ -771,9 +768,10 @@
             VMEM((WIDTH, 128), BF16),
             VMEM((128, WIDTH), BF16),
             VMEM((128, WIDTH), F32),
-            DMA((16,)), DMA((4, 4)), DMA((4, 4)), DMA((8, 4)), DMA((2,)),
-            DMA((2, 2, 4)), DMA((2,)), DMA((6, 4)), DMA((8, 4)), DMA((2, 8)), DMA((8,)), DMA((11,)), DMA((6,)),
-            DMA((2, 4)), DMA((16, 4)), DMA((2,)), DMA((16,)), DMA((8, 2)), DMA((16,)), DMA((8,)),
+            DMA((16,)), DMA((1,)), DMA((1,)), DMA((4, 4)), DMA((4,)), DMA((2,)), DMA((2, 2)),
+            DMA((2,)), DMA((1,)), DMA((2,)), DMA((4,)), DMA((1,)), DMA((1,)), DMA((1,)), DMA((1,)),
+            DMA((2, 4)), DMA((8, 4)), DMA((4,)), DMA((2,)), DMA((4,)), DMA((1,)), DMA((4, 2)),
+            DMA((1,)), DMA((1,)), DMA((1,)),
         ],
         compiler_params=pltpu.CompilerParams(
             collective_id=1, has_side_effects=True, vmem_limit_bytes=56 * 2**20

time: 71.4 us -> 68.4 us (0.958)
  the two profiles are of different devices: /device:TPU:1 before, /device:TPU:57 now
where the time goes in v5:
time: 68.4 us; the launch traced here: 68.3 us
  Pallas kernels  68.3 us (100%)
    pallas_call x1, Pallas kernels, per_device(): pl.pallas_call(layer_kernel, out_shape=pltpu.VMEM((128, WIDTH), BF16), in...  67.5 us

profile of v5, /device:TPU:57, one launch (start us, length us, event | category | flops | bytes accessed | tf_op | source)
XLA Modules:
  0.0 68.3 jit_solution(2972647924593597807)
XLA Ops:
  0.0 67.5 %layer.1.rows = bf16[128,2048]{1,0:T(8,128)(2,1)S(1)} custom-call(bf16[1024,256]{1,0:T(8,128)(2,1)} %tokens.1, f32[1,2048]{1,0:T(1,128)} %bitcast.6, bf16[2048,128]{1,0:T(8,128)(2,1)} %wq.1, bf16[2048,128]{1,0:T(8,128)(2,1)} %wk.1, bf16[2048,128]{1,0:T(8,128)(2,1)} %wv.1, bf16[2048,128]{1,0:T(8,128)(2,1)} %wo.1, bf16[2048,128]{1,0:T(8,128)(2,1)} %wi.1, ...), custom_call_target="tpu_custom_call" | custom-call | tf_op jit(solution)/shard_map/layer/pallas_call | solution.py:732
  67.5 0.8 %store.1 = bf16[128,2048]{1,0:T(8,128)(2,1)} custom-call(bf16[128,2048]{1,0:T(8,128)(2,1)S(1)} %layer.1.rows), custom_call_target="tpu_custom_call" | custom-call | tf_op jit(solution)/shard_map/store/pallas_call | solution.py:786

commit v6 on v5

--- a/solution.py
+++ b/solution.py
@@ -65,6 +65,22 @@
 
     mine = local(tokens, xbuf.at[tp], lsem.at[0])
     mine.start()
+    barrier = pltpu.get_barrier_semaphore()
+    columns = [((z + step) % 4) * 4 + y for step in range(4)]
+    ranks = [(tp + step) % 8 for step in range(8)]
+    for n in range(1, 32):
+        pl.semaphore_signal(
+            barrier, inc=1, device_id={"sp": columns[n // 8], "tp": ranks[n % 8]},
+            device_id_type=MESH,
+        )
+    for step in (1, 3):
+        pl.semaphore_signal(
+            barrier, inc=1, device_id=dev(z, (y + step) % 4, x, c), device_id_type=MESH
+        )
+    for step in (1, 15):
+        pl.semaphore_signal(
+            barrier, inc=1, device_id={"sp": (sp + step) % 16, "tp": tp}, device_id_type=MESH
+        )
     weights = [
         local(w, wtmp.at[n], lsem.at[1 + n]) for n, w in enumerate((wq, wk, wv, wo, wi, wx))
     ]
@@ -86,25 +102,6 @@
         w.start()
     out_a.start()
     out_c.start()
-    barrier = pltpu.get_barrier_semaphore()
-
-    def greet(step, carry):
-        other = (z * 8 + tp + step) % 32
-        pl.semaphore_signal(
-            barrier, inc=1, device_id={"sp": (other // 8) * 4 + y, "tp": other % 8},
-            device_id_type=MESH,
-        )
-        return carry
-
-    lax.fori_loop(1, 32, greet, 0)
-    for step in (1, 3):
-        pl.semaphore_signal(
-            barrier, inc=1, device_id=dev(z, (y + step) % 4, x, c), device_id_type=MESH
-        )
-    for step in (1, 15):
-        pl.semaphore_signal(
-            barrier, inc=1, device_id={"sp": (sp + step) % 16, "tp": tp}, device_id_type=MESH
-        )
     mine.wait()
     pl.semaphore_wait(barrier, 35)
 
@@ -173,22 +170,21 @@
 
     def z_sends(n):
         at = pl.ds(pl.multiple_of(n * CHUNK, CHUNK), CHUNK)
-        for i in range(2):
-            zt = 2 * c + i
-            own = (zt == z) & (zc == c)
-            pieces = (
-                (kvout.at[i, :, at], kvbuf.at[sp, :, at], kvrecv.at[native(sp), n]),
-                (qout.at[i, :, at], qbuf.at[qslot, pl.ds(0, QROWS), at], qrecv.at[qslot, n]),
-            )
-
-            @pl.when(own)
-            def _():
-                for src, dst, recv in pieces:
+        for k in range(2):
+            for i in range(2):
+                zt = 2 * c + i
+                own = (zt == z) & (zc == c)
+                src, dst, recv = (
+                    (kvout.at[i, :, at], kvbuf.at[sp, :, at], kvrecv.at[native(sp), n]),
+                    (qout.at[i, :, at], qbuf.at[qslot, pl.ds(0, QROWS), at], qrecv.at[qslot, n]),
+                )[k]
+
+                @pl.when(own)
+                def _():
                     local(src, dst, recv).start()
 
-            @pl.when(jnp.logical_not(own))
-            def _():
-                for k, (src, dst, recv) in enumerate(pieces):
+                @pl.when(jnp.logical_not(own))
+                def _():
                     remote(src, dst, zsend.at[i, k], recv, dev(zt, y, x, zc)).start()
 
     for i in range(2):

time: 68.4 us -> 68.3 us (level)
  no operation moved by 1% of the time
where the time goes in v6:
time: 68.3 us; the launch traced here: 68.2 us
  Pallas kernels  68.2 us (100%)
    pallas_call x1, Pallas kernels, per_device(): pl.pallas_call(layer_kernel, out_shape=pltpu.VMEM((128, WIDTH), BF16), in...  67.4 us

profile of v6, /device:TPU:57, one launch (start us, length us, event | category | flops | bytes accessed | tf_op | source)
XLA Modules:
  0.0 68.2 jit_solution(13628742821400850894)
XLA Ops:
  0.0 67.4 %layer.1.rows = bf16[128,2048]{1,0:T(8,128)(2,1)S(1)} custom-call(bf16[1024,256]{1,0:T(8,128)(2,1)} %tokens.1, f32[1,2048]{1,0:T(1,128)} %bitcast.6, bf16[2048,128]{1,0:T(8,128)(2,1)} %wq.1, bf16[2048,128]{1,0:T(8,128)(2,1)} %wk.1, bf16[2048,128]{1,0:T(8,128)(2,1)} %wv.1, bf16[2048,128]{1,0:T(8,128)(2,1)} %wo.1, bf16[2048,128]{1,0:T(8,128)(2,1)} %wi.1, ...), custom_call_target="tpu_custom_call" | custom-call | tf_op jit(solution)/shard_map/layer/pallas_call | solution.py:728
  67.4 0.8 %store.1 = bf16[128,2048]{1,0:T(8,128)(2,1)} custom-call(bf16[128,2048]{1,0:T(8,128)(2,1)S(1)} %layer.1.rows), custom_call_target="tpu_custom_call" | custom-call | tf_op jit(solution)/shard_map/store/pallas_call | solution.py:782
